TPU v7x, 256 devices: a 4x2x16 block of a 4x16x16 slice. The times are simulated.
256 devices in a mesh: grp: 2 (over y), kv: 16 (over z), tp: 8 (over x, core).
Axes of the slice: x: 4, y: 2, z: 16, core: 2. Of those that a mesh axis runs over, the one named last changes fastest.
The devices are a block of a 4x16x16 slice.
Arguments:
- residual: bfloat16 [32, 4096], P('grp', ('kv', 'tp')), parts along dimension 0, may hold values from -11 to 11
- cache_keys: bfloat16 [32, 16384, 8, 128], P('grp', 'kv', 'tp'), parts along dimension 0, may hold values from -210 to 210
- cache_values: bfloat16 [32, 16384, 8, 128], P('grp', 'kv', 'tp'), parts along dimension 0, may hold values from -6 to 6
- norm_gain: bfloat16 [4096], P('kv'), may hold values from 0.099609375 to 1.8984375
- query_weight: bfloat16 [4096, 2048], P('kv', 'tp'), may hold values from -0.09375 to 0.09375
- key_weight: bfloat16 [4096, 1024], P('kv', 'tp'), may hold values from -0.25 to 0.25
- value_weight: bfloat16 [4096, 1024], P('kv', 'tp'), may hold values from -0.375 to 0.375
- head_lambda: float32 [16], P('tp'), may hold values from 0.3 to 0.8
- head_gain: bfloat16 [128], replicated, may hold values from 0.099609375 to 1.8984375
- out_weight: bfloat16 [2048, 4096], P('tp', 'kv'), may hold values from -0.1875 to 0.1875
- mixer_gain: bfloat16 [4096], P('kv'), may hold values from 0.099609375 to 1.8984375
- up_weight: bfloat16 [4096, 16384], P('kv', 'tp'), may hold values from -0.09375 to 0.09375
- down_weight: bfloat16 [16384, 4096], P('tp', 'kv'), may hold values from -0.0625 to 0.0625
Outputs:
- updated: bfloat16 [32, 4096], P('grp', ('kv', 'tp')), parts along dimension 0
There are 2 independent parts, one for each index of `grp`. A program takes and returns all parts, laid end to end along the dimension named above; an argument that names none is the same for every part. Nothing has to cross between parts.
All inputs are finite; a program needn't handle non-finite values.
Results may differ from a plain program's by a relative error of at most 0.018.
Values may be sent and summed in bfloat16 or wider, within the bound.
A program may use at most 64 MiB of HBM per device.

v0:
```python
import jax
import jax.numpy as jnp
from jax import lax
from jax.sharding import PartitionSpec as P

D = 4096
HEADS = 16
KV_HEADS = 8
HALF = 64
VDIM = 128


EPS = 1e-06


def in_order(parts, dim):
    parts = jnp.moveaxis(parts, 0, dim)
    lengths = parts.shape
    return parts.reshape(*lengths[:dim], lengths[dim] * lengths[dim + 1], *lengths[dim + 2 :])


def sent_to_all(shard, axis):
    devices = lax.axis_size(axis)
    return lax.all_to_all(
        jnp.broadcast_to(shard[None], (devices, *shard.shape)), axis, 0, 0, tiled=True
    )


def gathered_copies(shard, axis, dim):
    return in_order(sent_to_all(shard, axis), dim)


def of_everyone(shard, axis):
    everything = sent_to_all(shard, axis)
    return jnp.sum(everything, axis=0)


def together(arrays, axis):
    ravelled, at, finished = (jnp.concatenate([a.reshape(-1) for a in arrays]), 0, [])
    so_far = of_everyone(ravelled, axis)
    for a in arrays:
        finished.append(so_far[at : at + a.size].reshape(a.shape))
        at += a.size
    return tuple(finished)


def collected_together(shard, axis):
    leaves = jax.tree.leaves(shard)
    order = sorted(range(len(leaves)), key=lambda k: -leaves[k].size)
    width = (1, *leaves[order[0]].shape)[-1]
    lines = [
        jnp.pad(leaves[k].reshape(-1), (0, -leaves[k].size % width)).reshape(-1, width)
        for k in order
    ]
    both, at, found = (sent_to_all(jnp.concatenate(lines), axis), 0, {})
    for k, line in zip(order, lines):
        section = both[:, at : at + len(line)].reshape(len(both), -1)
        found[k] = section[:, : leaves[k].size].reshape(-1, *leaves[k].shape)
        at += len(line)
    numbers = iter(range(len(leaves)))
    return jax.tree.map(lambda _: found[next(numbers)], shard)


def joined_by_halves(pieces, combine):
    while len(jax.tree.leaves(pieces)[0]) > 1:
        pieces = jax.vmap(combine)(
            *(jax.tree.map(lambda part: part[side::2], pieces) for side in (0, 1))
        )
    return jax.tree.map(lambda part: part[0], pieces)


def joined_all(shard, axis, combine):
    pieces = collected_together(shard, axis)
    return joined_by_halves(pieces, combine)


def cut_along(shard, dim, devices):
    lengths = shard.shape
    parts = shard.reshape(*lengths[:dim], devices, lengths[dim] // devices, *lengths[dim + 1 :])
    return jnp.moveaxis(parts, dim, 0)


def sum_at_owner(shard, axis, dim):
    devices = lax.axis_size(axis)
    parts = lax.all_to_all(cut_along(shard, dim, devices), axis, 0, 0, tiled=True)
    return jnp.sum(parts, axis=0)


def combine(first, second):
    top = jnp.maximum(first[0], second[0])
    left = jnp.exp(first[0] - top)
    right = jnp.exp(second[0] - top)
    return (
        top,
        first[1] * left + second[1] * right,
        first[2] * left[..., None] + second[2] * right[..., None],
    )


def body(
    residual,
    cache_keys,
    cache_values,
    norm_gain,
    query_weight,
    key_weight,
    value_weight,
    head_lambda,
    head_gain,
    out_weight,
    mixer_gain,
    up_weight,
    down_weight,
):
    f32 = jnp.float32
    bf16 = jnp.bfloat16
    rows = residual.shape[0]
    kv_local = cache_keys.shape[2]
    group = HEADS // KV_HEADS
    scale = 1.0 / HALF**0.5
    block = gathered_copies(residual, "tp", 1).astype(f32)
    scaled = (block * norm_gain.astype(f32)).astype(bf16)
    q_part = jnp.dot(scaled, query_weight, preferred_element_type=f32)
    k_part = jnp.dot(scaled, key_weight, preferred_element_type=f32)
    v_part = jnp.dot(scaled, value_weight, preferred_element_type=f32)
    sq_part = jnp.sum(block * block, axis=1)
    q_sum, k_sum, v_sum, sq_sum = together((q_part, k_part, v_part, sq_part), "kv")
    inv_rms = lax.rsqrt(sq_sum / D + EPS)[:, None]
    query = (inv_rms * q_sum).astype(bf16).reshape(rows, kv_local, group, 2, HALF)
    new_key = (inv_rms * k_sum).astype(bf16).reshape(rows, kv_local, 2, HALF)
    new_value = (inv_rms * v_sum).astype(bf16).reshape(rows, kv_local, VDIM)
    positions = cache_keys.shape[1]
    keys = cache_keys.reshape(rows, positions, kv_local, 2, HALF)
    scores = jnp.einsum("bkgch,bpkch->bkgcp", query, keys, preferred_element_type=f32) * scale
    local_top = jnp.max(scores, axis=4)
    expo = jnp.exp(scores - local_top[..., None])
    local_total = jnp.sum(expo, axis=4)
    local_weighted = jnp.einsum(
        "bkgcp,bpkv->bkgcv", expo.astype(bf16), cache_values, preferred_element_type=f32
    )
    cache_top, total, weighted = joined_all((local_top, local_total, local_weighted), "kv", combine)
    own = jnp.einsum("bkgch,bkch->bkgc", query, new_key, preferred_element_type=f32) * scale
    top = jnp.maximum(cache_top, own)
    old_part = jnp.exp(cache_top - top)
    own_part = jnp.exp(own - top)
    numer = (
        weighted * old_part[..., None]
        + own_part[..., None] * new_value.astype(f32)[:, :, None, None, :]
    )
    attended = numer / (total * old_part + own_part)[..., None]
    lambdas = head_lambda.reshape(kv_local, group)[None, :, :, None]
    diff = attended[:, :, :, 0] - lambdas * attended[:, :, :, 1]
    normed = (
        diff * lax.rsqrt(jnp.mean(diff * diff, axis=3, keepdims=True) + EPS) * head_gain.astype(f32)
    )
    heads_out = normed.astype(bf16).reshape(rows, kv_local * group * VDIM)
    projected = jnp.dot(heads_out, out_weight, preferred_element_type=f32)
    mixed = (residual.astype(f32) + sum_at_owner(projected, "tp", 1)).astype(bf16)
    mixed_block = gathered_copies(mixed, "tp", 1).astype(f32)
    scaled2 = (mixed_block * mixer_gain.astype(f32)).astype(bf16)
    up_part = jnp.dot(scaled2, up_weight, preferred_element_type=f32)
    sq_mixed = jnp.sum(mixed_block * mixed_block, axis=1)
    up_share = sum_at_owner(up_part, "kv", 1)
    sq_total = of_everyone(sq_mixed, "kv")
    inv_rms2 = lax.rsqrt(sq_total / D + EPS)[:, None]
    share = jnp.square(jnp.maximum(inv_rms2 * up_share, 0.0)).astype(bf16)
    hidden = gathered_copies(share, "kv", 1)
    down_part = jnp.dot(hidden, down_weight, preferred_element_type=f32)
    return (mixed.astype(f32) + sum_at_owner(down_part, "tp", 1)).astype(bf16)


def solution(mesh):
    in_specs = (
        P("grp", ("kv", "tp")),
        P("grp", "kv", "tp", None),
        P("grp", "kv", "tp", None),
        P("kv"),
        P("kv", "tp"),
        P("kv", "tp"),
        P("kv", "tp"),
        P("tp"),
        P(),
        P("tp", "kv"),
        P("kv"),
        P("kv", "tp"),
        P("tp", "kv"),
    )
    out_specs = P("grp", ("kv", "tp"))
    return jax.shard_map(body, mesh=mesh, in_specs=in_specs, out_specs=out_specs, check_vma=False)
```

profile of v0, /device:TPU:33, one launch (start us, length us, event | category | flops | bytes accessed | tf_op | source)
XLA Modules:
  0.0 212.6 jit_solution(8546478358482389014)
XLA Ops:
  1.4 23.6 %all-to-all-start = ((bf16[8,2,256]{2,1,0:T(2,128)(2,1)}), bf16[8,2,256]{2,1,0:T(2,128)(2,1)S(1)}, u32[]{:S(2)}, u32[]{:S(2)}) async-start(bf16[8,2,256]{2,1,0:T(2,128)(2,1)} %reshape.395), calls=%async_computation | async-start | bytes 16384 | tf_op jit(solution)/shard_map/all_to_all | solution.py:24
  25.7 4.0 %all-to-all-done = bf16[8,2,256]{2,1,0:T(2,128)(2,1)S(1)} async-done(((bf16[8,2,256]{2,1,0:T(2,128)(2,1)}), bf16[8,2,256]{2,1,0:T(2,128)(2,1)S(1)}, u32[]{:S(2)}, u32[]{:S(2)}) %all-to-all-start) | async-done | bytes 8224 | tf_op jit(solution)/shard_map/all_to_all | solution.py:24
  32.2 1.1 broadcast_in_dim.13
  33.3 6.0 %all-to-all-start.1 = ((f32[16,1,8208]{2,1,0:T(1,128)}), f32[16,1,8208]{2,1,0:T(1,128)S(1)}, u32[]{:S(2)}, u32[]{:S(2)}) async-start(f32[16,1,8208]{2,1,0:T(1,128)} %broadcast_in_dim.13), calls=%async_computation.1 | async-start | bytes 1064960 | tf_op jit(solution)/shard_map/all_to_all | solution.py:24
  39.3 6.4 %copy.174 = bf16[16,1024,1,128]{1,3,0,2:T(8,128)(2,1)} copy(bf16[16,1024,1,128]{3,1,2,0:T(8,128)(2,1)} %param.14) | data formatting | bytes 8388608 | tf_op args[1]
  45.7 16.7 %all-to-all-done.1 = f32[16,1,8208]{2,1,0:T(1,128)S(1)} async-done(((f32[16,1,8208]{2,1,0:T(1,128)}), f32[16,1,8208]{2,1,0:T(1,128)S(1)}, u32[]{:S(2)}, u32[]{:S(2)}) %all-to-all-start.1) | async-done | bytes 525344 | tf_op jit(solution)/shard_map/all_to_all | solution.py:24
  62.9 2.9 %fusion.43 = (f32[16,2,2]{1,2,0:T(2,128)S(1)}, f32[16,1,2,2,1024]{4,2,3,0,1:T(2,128)S(1)}) fusion(bf16[16,1024,2,64]{1,3,2,0:T(8,128)(2,1)} %bitcast.142, bf16[16,2,2,64]{3,2,1,0:T(2,128)(2,1)S(1)} %multiply_convert_fusion), kind=kOutput, calls=%fused_computation.95 | convolution fusion | flops 8519616 | bytes 4464896 | tf_op jit(solution)/shard_map/bkgch,bpkch->bkgcp/dot_general | solution.py:134
  66.9 3.0 %fusion = f32[16,2,2,128]{3,1,2,0:T(2,128)S(1)} fusion(bf16[16,1024,1,128]{3,1,2,0:T(8,128)(2,1)} %param.15, f32[16,1,2,2,1024]{4,2,3,0,1:T(2,128)S(1)} %get-tuple-element.30, f32[16,2,2]{1,2,0:T(2,128)S(1)} %get-tuple-element.29), kind=kOutput, calls=%fused_computation | convolution fusion | flops 16908288 | bytes 4489472 | tf_op jit(solution)/shard_map/bkgcp,bpkv->bkgcv/dot_general | solution.py:138
  70.8 12.7 %all-to-all-start.2 = ((f32[16,66,128]{2,1,0:T(8,128)}), f32[16,66,128]{2,1,0:T(8,128)S(1)}, u32[]{:S(2)}, u32[]{:S(2)}) async-start(f32[16,66,128]{2,1,0:T(8,128)} %broadcast_in_dim.14), calls=%async_computation.2 | async-start | bytes 1179648 | tf_op jit(solution)/shard_map/all_to_all | solution.py:24
  84.2 24.4 %all-to-all-done.2 = f32[16,66,128]{2,1,0:T(8,128)S(1)} async-done(((f32[16,66,128]{2,1,0:T(8,128)}), f32[16,66,128]{2,1,0:T(8,128)S(1)}, u32[]{:S(2)}, u32[]{:S(2)}) %all-to-all-start.2) | async-done | bytes 540704 | tf_op jit(solution)/shard_map/all_to_all | solution.py:24
  108.7 1.5 slice.117
  110.3 1.5 slice.118
  111.9 1.5 slice.136
  113.4 1.5 slice.137
  123.1 13.5 %all_to_all.47 = f32[8,1,512]{2,1,0:T(1,128)S(1)} all-to-all(f32[8,1,512]{2,1,0:T(1,128)S(1)} %reshape.397), channel_id=1, replica_groups=mesh['grp'=2,'kv'=16,'tp'=8] {'tp'}, dimensions={0} | all-to-all | bytes 32768 | tf_op jit(solution)/shard_map/all_to_all | solution.py:85
  138.6 3.9 %all-to-all-start.4 = ((bf16[8,2,256]{2,1,0:T(2,128)(2,1)}), bf16[8,2,256]{2,1,0:T(2,128)(2,1)S(1)}, u32[]{:S(2)}, u32[]{:S(2)}) async-start(bf16[8,2,256]{2,1,0:T(2,128)(2,1)} %reshape.399), calls=%async_computation.4 | async-start | bytes 16384 | tf_op jit(solution)/shard_map/all_to_all | solution.py:24
  143.2 4.1 %all-to-all-done.4 = bf16[8,2,256]{2,1,0:T(2,128)(2,1)S(1)} async-done(((bf16[8,2,256]{2,1,0:T(2,128)(2,1)}), bf16[8,2,256]{2,1,0:T(2,128)(2,1)S(1)}, u32[]{:S(2)}, u32[]{:S(2)}) %all-to-all-start.4) | async-done | bytes 8224 | tf_op jit(solution)/shard_map/all_to_all | solution.py:24
  148.2 7.3 %all-to-all-start.5 = ((f32[16,1,16]{2,1,0:T(1,128)}), f32[16,1,16]{2,1,0:T(1,128)S(1)}, u32[]{:S(2)}, u32[]{:S(2)}) async-start(f32[16,1,16]{2,1,0:T(1,128)} %broadcast_in_dim.16), calls=%async_computation.5 | async-start | bytes 16384 | tf_op jit(solution)/shard_map/all_to_all | solution.py:24
  156.5 10.1 %all-to-all-done.5 = f32[16,1,16]{2,1,0:T(1,128)S(1)} async-done(((f32[16,1,16]{2,1,0:T(1,128)}), f32[16,1,16]{2,1,0:T(1,128)S(1)}, u32[]{:S(2)}, u32[]{:S(2)}) %all-to-all-start.5) | async-done | bytes 1056 | tf_op jit(solution)/shard_map/all_to_all | solution.py:24
  166.6 4.0 %all-to-all-start.6 = ((f32[16,16,128]{2,1,0:T(8,128)}), f32[16,16,128]{2,1,0:T(8,128)S(1)}, u32[]{:S(2)}, u32[]{:S(2)}) async-start(f32[16,16,128]{2,1,0:T(8,128)} %convolution_bitcast_fusion), calls=%async_computation.6 | async-start | bytes 262144 | tf_op jit(solution)/shard_map/all_to_all | solution.py:85
  170.6 11.5 %all-to-all-done.6 = f32[16,16,128]{2,1,0:T(8,128)S(1)} async-done(((f32[16,16,128]{2,1,0:T(8,128)}), f32[16,16,128]{2,1,0:T(8,128)S(1)}, u32[]{:S(2)}, u32[]{:S(2)}) %all-to-all-start.6) | async-done | bytes 131104 | tf_op jit(solution)/shard_map/all_to_all | solution.py:85
  182.9 5.5 %all-to-all-start.7 = ((bf16[16,16,128]{2,1,0:T(8,128)(2,1)}), bf16[16,16,128]{2,1,0:T(8,128)(2,1)S(1)}, u32[]{:S(2)}, u32[]{:S(2)}) async-start(bf16[16,16,128]{2,1,0:T(8,128)(2,1)} %broadcast_in_dim.17), calls=%async_computation.7 | async-start | bytes 131072 | tf_op jit(solution)/shard_map/all_to_all | solution.py:24
  189.1 10.7 %all-to-all-done.7 = bf16[16,16,128]{2,1,0:T(8,128)(2,1)S(1)} async-done(((bf16[16,16,128]{2,1,0:T(8,128)(2,1)}), bf16[16,16,128]{2,1,0:T(8,128)(2,1)S(1)}, u32[]{:S(2)}, u32[]{:S(2)}) %all-to-all-start.7) | async-done | bytes 65568 | tf_op jit(solution)/shard_map/all_to_all | solution.py:24
  200.7 10.4 %all_to_all.48 = f32[8,1,512]{2,1,0:T(1,128)S(1)} all-to-all(f32[8,1,512]{2,1,0:T(1,128)S(1)} %reshape.401), channel_id=1, replica_groups=mesh['grp'=2,'kv'=16,'tp'=8] {'tp'}, dimensions={0} | all-to-all | bytes 32768 | tf_op jit(solution)/shard_map/all_to_all | solution.py:85
  (131 shorter events, 23.9 us)
Async XLA Ops:
  0.0 30.1 %copy-start = (bf16[256,256]{1,0:T(8,128)(2,1)S(1)}, bf16[256,256]{1,0:T(8,128)(2,1)}, u32[]{:S(2)}) copy-start(bf16[256,256]{1,0:T(8,128)(2,1)} %param.17) | copy-start | bytes 393220
  1.4 28.3 %all-to-all-start = ((bf16[8,2,256]{2,1,0:T(2,128)(2,1)}), bf16[8,2,256]{2,1,0:T(2,128)(2,1)S(1)}, u32[]{:S(2)}, u32[]{:S(2)}) async-start(bf16[8,2,256]{2,1,0:T(2,128)(2,1)} %reshape.395), calls=%async_computation | async-start | bytes 16384 | tf_op jit(solution)/shard_map/all_to_all | solution.py:24
  33.3 29.1 %all-to-all-start.1 = ((f32[16,1,8208]{2,1,0:T(1,128)}), f32[16,1,8208]{2,1,0:T(1,128)S(1)}, u32[]{:S(2)}, u32[]{:S(2)}) async-start(f32[16,1,8208]{2,1,0:T(1,128)} %broadcast_in_dim.13), calls=%async_computation.1 | async-start | bytes 1064960 | tf_op jit(solution)/shard_map/all_to_all | solution.py:24
  65.8 17.7 %copy-start.7 = (bf16[128]{0:T(256)(128)(2,1)S(1)}, bf16[128]{0:T(256)(128)(2,1)}, u32[]{:S(2)}) copy-start(bf16[128]{0:T(256)(128)(2,1)} %param.21) | copy-start | bytes 772
  65.9 17.7 %copy-start.3 = (bf16[256,256]{1,0:T(8,128)(2,1)S(1)}, bf16[256,256]{1,0:T(8,128)(2,1)}, u32[]{:S(2)}) copy-start(bf16[256,256]{1,0:T(8,128)(2,1)} %param.22) | copy-start | bytes 393220
  70.8 37.8 %all-to-all-start.2 = ((f32[16,66,128]{2,1,0:T(8,128)}), f32[16,66,128]{2,1,0:T(8,128)S(1)}, u32[]{:S(2)}, u32[]{:S(2)}) async-start(f32[16,66,128]{2,1,0:T(8,128)} %broadcast_in_dim.14), calls=%async_computation.2 | async-start | bytes 1179648 | tf_op jit(solution)/shard_map/all_to_all | solution.py:24
  83.5 39.0 %copy-start.5 = (f32[2]{0:T(128)S(1)}, f32[2]{0:T(128)}, u32[]{:S(2)}) copy-start(f32[2]{0:T(128)} %param.20) | copy-start | bytes 28
  83.5 54.4 %copy-start.4 = (bf16[16,32]{1,0:T(8,128)(2,1)S(1)}, bf16[16,32]{1,0:T(8,128)(2,1)}, u32[]{:S(2)}) copy-start(bf16[16,32]{1,0:T(8,128)(2,1)} %param.13) | copy-start | bytes 3076
  83.7 58.9 %copy-start.6 = (bf16[256]{0:T(256)(128)(2,1)S(1)}, bf16[256]{0:T(256)(128)(2,1)}, u32[]{:S(2)}) copy-start(bf16[256]{0:T(256)(128)(2,1)} %param.23) | copy-start | bytes 1540
  83.7 59.0 %copy-start.1 = (bf16[256,2048]{1,0:T(8,128)(2,1)S(1)}, bf16[256,2048]{1,0:T(8,128)(2,1)}, u32[]{:S(2)}) copy-start(bf16[256,2048]{1,0:T(8,128)(2,1)} %param.24) | copy-start | bytes 3145732
  116.8 71.6 %copy-start.2 = (bf16[2048,256]{1,0:T(8,128)(2,1)S(1)}, bf16[2048,256]{1,0:T(8,128)(2,1)}, u32[]{:S(2)}) copy-start(bf16[2048,256]{1,0:T(8,128)(2,1)} %param.25) | copy-start | bytes 3145732
  138.6 8.6 %all-to-all-start.4 = ((bf16[8,2,256]{2,1,0:T(2,128)(2,1)}), bf16[8,2,256]{2,1,0:T(2,128)(2,1)S(1)}, u32[]{:S(2)}, u32[]{:S(2)}) async-start(bf16[8,2,256]{2,1,0:T(2,128)(2,1)} %reshape.399), calls=%async_computation.4 | async-start | bytes 16384 | tf_op jit(solution)/shard_map/all_to_all | solution.py:24
  148.2 18.5 %all-to-all-start.5 = ((f32[16,1,16]{2,1,0:T(1,128)}), f32[16,1,16]{2,1,0:T(1,128)S(1)}, u32[]{:S(2)}, u32[]{:S(2)}) async-start(f32[16,1,16]{2,1,0:T(1,128)} %broadcast_in_dim.16), calls=%async_computation.5 | async-start | bytes 16384 | tf_op jit(solution)/shard_map/all_to_all | solution.py:24
  166.6 15.5 %all-to-all-start.6 = ((f32[16,16,128]{2,1,0:T(8,128)}), f32[16,16,128]{2,1,0:T(8,128)S(1)}, u32[]{:S(2)}, u32[]{:S(2)}) async-start(f32[16,16,128]{2,1,0:T(8,128)} %convolution_bitcast_fusion), calls=%async_computation.6 | async-start | bytes 262144 | tf_op jit(solution)/shard_map/all_to_all | solution.py:85
  182.9 16.9 %all-to-all-start.7 = ((bf16[16,16,128]{2,1,0:T(8,128)(2,1)}), bf16[16,16,128]{2,1,0:T(8,128)(2,1)S(1)}, u32[]{:S(2)}, u32[]{:S(2)}) async-start(bf16[16,16,128]{2,1,0:T(8,128)(2,1)} %broadcast_in_dim.17), calls=%async_computation.7 | async-start | bytes 131072 | tf_op jit(solution)/shard_map/all_to_all | solution.py:24
where the time goes:
time: 214 us; the launch traced here: 213 us
  waiting for transfers between devices  81.5 us (38%)
  starting transfers between devices  63.1 us (29%)
  local copies, waits for them, and re-layouts  27.8 us (13%)
  blocking collectives  23.9 us (11%)
  matrix products  10.2 us (5%)
  other arithmetic  5.41 us (3%)
    all_to_all x6, waiting for transfers between devices, sent_to_all(): lax.all_to_all(jnp.broadcast_to(shard[None], (devices, *shard.shape)), ax...  70 us
    all_to_all x6, starting transfers between devices, sent_to_all(): lax.all_to_all(jnp.broadcast_to(shard[None], (devices, *shard.shape)), ax...  59.1 us
    all_to_all x2, blocking collectives, sum_at_owner(): lax.all_to_all(cut_along(shard, dim, devices), axis, 0, 0, tiled=True)  23.9 us
    all_to_all x1, waiting for transfers between devices, sum_at_owner(): lax.all_to_all(cut_along(shard, dim, devices), axis, 0, 0, tiled=True)  11.5 us
    slice x10, local copies, waits for them, and re-layouts, joined_by_halves(): part[side::2]  10.4 us
    unnamed x35, local copies, waits for them, and re-layouts  10 us
  transfers between devices with their start and end apart: 7, of which 7 were waited for; matrix products, arithmetic and copies ran while one was open for 5% of the time, Pallas kernels for 0%

commit v1 on v0

v1 whole, which is shorter than its diff:
```python
import functools

import jax
import jax.numpy as jnp
from jax import lax
from jax.experimental import pallas as pl
from jax.experimental.pallas import tpu as pltpu
from jax.sharding import PartitionSpec as P

EPS = 1e-06
MESH = pl.DeviceIdType.MESH
F32 = jnp.float32
BF16 = jnp.bfloat16
LANES = 128
LOW = -1e30


def far_first(n):
    order = [n // 2]
    for k in range(1, n // 2 + 1):
        for d in (n // 2 - k, n // 2 + k):
            if 0 < d < n:
                order.append(d)
    return order


def iota(shape, dim):
    return lax.broadcasted_iota(jnp.int32, shape, dim)


def dot(a, b):
    return jnp.dot(a, b, preferred_element_type=F32)


def to_lanes(column):
    wide = jnp.broadcast_to(column, (column.shape[0], LANES))
    diagonal = iota(wide.shape, 0) == iota(wide.shape, 1)
    return jnp.sum(jnp.where(diagonal, wide, 0.0), axis=0, keepdims=True)


def to_rows(row, rows):
    wide = jnp.broadcast_to(row, (rows, LANES))
    diagonal = iota(wide.shape, 0) == iota(wide.shape, 1)
    return jnp.sum(jnp.where(diagonal, wide, 0.0), axis=1, keepdims=True)


def kernel(
    KV,
    TP,
    res_h,
    keys_h,
    values_h,
    ng_h,
    wq_h,
    wk_h,
    wv_h,
    lam_h,
    hg_h,
    wo_h,
    mg_h,
    wu_h,
    wd_h,
    out_ref,
    res,
    keys,
    values,
    ng,
    wp,
    lam,
    hg,
    wo,
    mg,
    wu,
    wd,
    abuf,
    qbuf,
    kvs,
    kvr,
    wbuf,
    mlbuf,
    dbuf,
    sqbuf,
    us,
    ur,
    hbuf,
    fs,
    fr,
    load_sem,
    a_send,
    a_recv,
    q_send,
    q_recv,
    r_send,
    r_recv,
    w_send,
    w_recv,
    m_send,
    m_recv,
    d_send,
    d_recv,
    s_send,
    s_recv,
    u_send,
    u_recv,
    h_send,
    h_recv,
    f_send,
    f_recv,
):
    z = lax.axis_index("kv")
    t = lax.axis_index("tp")
    rows = res_h.shape[0]
    piece = res_h.shape[1]
    per_tile = LANES // piece
    width = wo.shape[1]
    D = KV * width
    qcols = wq_h.shape[1]
    heads = qcols // LANES
    half = LANES // 2
    maps = heads * 2
    lines = rows * maps

    def load(src, dst, k):
        copy = pltpu.make_async_copy(src, dst, load_sem.at[k])
        copy.start()
        return copy

    ld_res = load(res_h, res, 0)
    for u in range(1, TP):
        peer = lax.rem(t + u, TP)
        pl.semaphore_signal(
            pltpu.get_barrier_semaphore(), inc=1, device_id={"tp": peer}, device_id_type=MESH
        )
    for u in far_first(KV):
        peer = lax.rem(z + u, KV)
        pl.semaphore_signal(
            pltpu.get_barrier_semaphore(), inc=1, device_id={"kv": peer}, device_id_type=MESH
        )
    ld_ng = load(ng_h, ng, 1)
    ld_wq = load(wq_h, wp.at[:, 0:qcols], 2)
    ld_wk = load(wk_h, wp.at[:, qcols : qcols + LANES], 3)
    ld_wv = load(wv_h, wp.at[:, qcols + LANES : qcols + 2 * LANES], 4)
    ld_keys = load(keys_h, keys, 5)
    ld_values = load(values_h, values, 6)
    ld_lam = load(lam_h, lam, 7)
    ld_hg = load(hg_h, hg, 8)
    ld_wo = load(wo_h, wo, 9)
    ld_mg = load(mg_h, mg, 10)
    ld_wu = load(wu_h, wu, 11)
    ld_wd = load(wd_h, wd, 12)

    started = []

    def send(src, dst, ssem, rsem, axis, peer):
        copy = pltpu.make_async_remote_copy(
            src_ref=src,
            dst_ref=dst,
            send_sem=ssem,
            recv_sem=rsem,
            device_id={axis: peer},
            device_id_type=MESH,
        )
        copy.start()
        started.append(copy)
        return copy

    kv_order = far_first(KV)
    tp_order = far_first(TP)

    def spread(src_of, dst, sems, rsems, axis):
        me, n, order = (z, KV, kv_order) if axis == "kv" else (t, TP, tp_order)
        copies = []
        for d in order:
            peer = lax.rem(me + d, n)
            copies.append(send(src_of(peer), dst.at[me], sems.at[d - 1], rsems.at[d - 1], axis, peer))
        return copies

    def arrive(copies):
        for copy in copies:
            copy.wait_recv()

    ld_res.wait()
    own_piece = res[...].astype(F32)
    tiled = jnp.concatenate([own_piece] * per_tile, axis=1)
    at = iota(tiled.shape, 1) // piece == lax.rem(t, per_tile)
    abuf[t] = jnp.where(at, tiled, 0.0).astype(BF16)
    pl.semaphore_wait(pltpu.get_barrier_semaphore(), TP - 1 + KV - 1)
    arrive(spread(lambda peer: abuf.at[t], abuf, a_send, a_recv, "tp"))
    block = jnp.concatenate(
        [
            sum(abuf[k * per_tile + j].astype(F32) for j in range(per_tile))
            for k in range(TP // per_tile)
        ],
        axis=1,
    )
    ld_ng.wait()
    gain = jnp.concatenate([ng[k : k + 1, :] for k in range(width // LANES)], axis=1).astype(F32)
    scaled = (block * gain).astype(BF16)
    ld_wq.wait()
    ld_wk.wait()
    ld_wv.wait()
    proj = dot(scaled, wp[...])
    qbuf[z] = proj[:, 0:qcols].astype(BF16)
    square = to_lanes(jnp.sum(block * block, axis=1, keepdims=True))
    for j in range(KV):
        kvs[j] = jnp.concatenate([proj[j : j + 1, qcols:], square], axis=1)
    kvr[z] = kvs[z]
    q_copies = spread(lambda peer: qbuf.at[z], qbuf, q_send, q_recv, "kv")
    r_copies = spread(lambda peer: kvs.at[peer], kvr, r_send, r_recv, "kv")
    arrive(q_copies)
    arrive(r_copies)
    q_sum = qbuf[0].astype(F32)
    r_sum = kvr[0]
    for j in range(1, KV):
        q_sum = q_sum + qbuf[j].astype(F32)
        r_sum = r_sum + kvr[j]
    inv_lanes = lax.rsqrt(r_sum[:, 2 * LANES :] / D + EPS)
    inv_own = jnp.sum(
        jnp.where(iota(inv_lanes.shape, 1) == z, inv_lanes, 0.0), axis=1, keepdims=True
    )
    new_key = (inv_own * r_sum[:, 0:LANES]).astype(BF16).astype(F32)
    new_value = (inv_own * r_sum[:, LANES : 2 * LANES]).astype(BF16).astype(F32)
    query = (to_rows(inv_lanes, rows) * q_sum).astype(BF16)

    pick = (iota((lines, rows), 0) // maps == iota((lines, rows), 1)).astype(BF16)
    spreadq = dot(pick, query)
    line = iota((lines, LANES), 0)
    chosen = spreadq[:, 0:LANES]
    for g in range(1, heads):
        chosen = jnp.where(
            lax.rem(line, maps) // 2 == g, spreadq[:, g * LANES : (g + 1) * LANES], chosen
        )
    mine = iota((lines, LANES), 1) // half == lax.rem(line, 2)
    lined = jnp.where(mine, chosen, 0.0) * (1.0 / half**0.5)

    ld_keys.wait()
    ld_values.wait()
    tops, totals, sums = [], [], []
    for p in range(lines // 8):
        seqs = 8 // maps
        qp = lined[8 * p : 8 * p + 8, :].astype(BF16)
        scores = None
        for k in range(seqs):
            part = lax.dot_general(
                qp, keys[seqs * p + k], (((1,), (1,)), ((), ())), preferred_element_type=F32
            )
            if scores is None:
                scores = part
            else:
                scores = jnp.where(iota(part.shape, 0) // maps == k, part, scores)
        top = jnp.max(scores, axis=1, keepdims=True)
        expo = jnp.exp(scores - top)
        total = jnp.sum(expo, axis=1, keepdims=True)
        probs = expo.astype(BF16)
        weighted = None
        for k in range(seqs):
            part = dot(probs, values[seqs * p + k])
            if weighted is None:
                weighted = part
            else:
                weighted = jnp.where(iota(part.shape, 0) // maps == k, part, weighted)
        tops.append(top)
        totals.append(total)
        sums.append(weighted)
    top = jnp.concatenate(tops, axis=0)
    total = jnp.concatenate(totals, axis=0)
    weighted = jnp.concatenate(sums, axis=0)
    own = jnp.sum(lined * new_key, axis=1, keepdims=True)
    own = jnp.where(iota(own.shape, 0) // maps == z, own, LOW)
    new_top = jnp.maximum(top, own)
    old_part = jnp.exp(top - new_top)
    own_part = jnp.exp(own - new_top)
    total = total * old_part + own_part
    weighted = weighted * old_part + own_part * new_value
    wbuf[z] = weighted.astype(BF16)
    lane = iota((lines, LANES), 1)
    both = jnp.where(lane == line, new_top, jnp.where(lane == line + half, total, 0.0))
    mlbuf[z] = jnp.sum(both, axis=0, keepdims=True)
    m_copies = spread(lambda peer: mlbuf.at[z], mlbuf, m_send, m_recv, "kv")
    w_copies = spread(lambda peer: wbuf.at[z], wbuf, w_send, w_recv, "kv")
    arrive(m_copies)
    ml = jnp.concatenate([mlbuf[j] for j in range(KV)], axis=0)
    shares = jnp.exp(ml - jnp.max(ml, axis=0, keepdims=True))
    grand = jnp.sum(shares * pltpu.roll(ml, half, 1), axis=0, keepdims=True)
    in_use = iota(ml.shape, 1) < half
    shares = jnp.where(in_use, shares / jnp.where(in_use[0:1], grand, 1.0), 0.0)
    columns = jnp.transpose(shares)
    arrive(w_copies)
    attended = columns[0:lines, 0:1] * wbuf[0].astype(F32)
    for j in range(1, KV):
        attended = attended + columns[0:lines, j : j + 1] * wbuf[j].astype(F32)
    ld_lam.wait()
    ld_hg.wait()
    lambdas = lam[0:1, 0:1]
    for g in range(1, heads):
        lambdas = jnp.where(
            lax.rem(iota((lines, 1), 0), maps) // 2 == g, lam[0:1, g : g + 1], lambdas
        )
    diff = attended - lambdas * pltpu.roll(attended, lines - 1, 0)
    normed = (
        diff
        * lax.rsqrt(jnp.mean(diff * diff, axis=1, keepdims=True) + EPS)
        * hg[...].astype(F32)
    ).astype(BF16)
    outs = []
    for g in range(heads):
        pick = iota((rows, lines), 1) == iota((rows, lines), 0) * maps + 2 * g
        outs.append(dot(pick.astype(BF16), normed))
    heads_out = jnp.concatenate(outs, axis=1).astype(BF16)
    ld_wo.wait()
    dbuf[t] = dot(heads_out, wo[...])
    arrive(spread(lambda peer: dbuf.at[t], dbuf, d_send, d_recv, "tp"))
    projected = dbuf[0]
    for j in range(1, TP):
        projected = projected + dbuf[j]
    mixed = (block + projected).astype(BF16).astype(F32)
    sqbuf[z] = to_lanes(jnp.sum(mixed * mixed, axis=1, keepdims=True))
    s_copies = spread(lambda peer: sqbuf.at[z], sqbuf, s_send, s_recv, "kv")
    ld_mg.wait()
    gain2 = jnp.concatenate([mg[k : k + 1, :] for k in range(width // LANES)], axis=1).astype(F32)
    scaled2 = (mixed * gain2).astype(BF16)
    ld_wu.wait()
    up = dot(scaled2, wu[...])
    share_width = up.shape[1] // KV
    for j in range(KV):
        us[j] = up[:, j * share_width : (j + 1) * share_width].astype(us.dtype)
    ur[z] = us[z]
    u_copies = spread(lambda peer: us.at[peer], ur, u_send, u_recv, "kv")
    arrive(s_copies)
    square2 = sqbuf[0]
    for j in range(1, KV):
        square2 = square2 + sqbuf[j]
    inv2 = to_rows(lax.rsqrt(square2 / D + EPS), rows)
    arrive(u_copies)
    up_sum = ur[0].astype(F32)
    for j in range(1, KV):
        up_sum = up_sum + ur[j].astype(F32)
    act = jnp.maximum(inv2 * up_sum, 0.0)
    hbuf[z] = (act * act).astype(BF16)
    arrive(spread(lambda peer: hbuf.at[z], hbuf, h_send, h_recv, "kv"))
    hidden = jnp.concatenate([hbuf[j] for j in range(KV)], axis=1)
    ld_wd.wait()
    down = dot(hidden, wd[...])
    for k in range(width // LANES):
        fs[k] = down[:, k * LANES : (k + 1) * LANES]
    fr[t] = fs[t // per_tile]
    arrive(spread(lambda peer: fs.at[peer // per_tile], fr, f_send, f_recv, "tp"))
    y = fr[0]
    for j in range(1, TP):
        y = y + fr[j]
    for k in range(width // LANES):
        y = y + jnp.where(t // per_tile == k, mixed[:, k * LANES : (k + 1) * LANES], 0.0)
    result = y[:, 0:piece]
    for k in range(1, per_tile):
        result = jnp.where(lax.rem(t, per_tile) == k, y[:, k * piece : (k + 1) * piece], result)
    out_ref[...] = result.astype(out_ref.dtype)
    for copy in started:
        copy.wait_send()


def body(
    KV,
    TP,
    residual,
    cache_keys,
    cache_values,
    norm_gain,
    query_weight,
    key_weight,
    value_weight,
    head_lambda,
    head_gain,
    out_weight,
    mixer_gain,
    up_weight,
    down_weight,
):
    rows, piece = residual.shape
    positions, depth = cache_keys.shape[1], cache_keys.shape[3]
    width = out_weight.shape[1]
    qcols = query_weight.shape[1]
    lines = rows * qcols * 2 // LANES
    share = up_weight.shape[1] // KV
    any_spec = pl.BlockSpec(memory_space=pl.ANY)
    dma = pltpu.SemaphoreType.DMA
    keys = cache_keys.reshape(rows, positions, depth)
    values = cache_values.reshape(rows, positions, depth)
    args = (
        residual,
        keys,
        values,
        norm_gain.reshape(width // LANES, LANES),
        query_weight,
        key_weight,
        value_weight,
        head_lambda.reshape(1, -1),
        head_gain.reshape(1, -1),
        out_weight,
        mixer_gain.reshape(width // LANES, LANES),
        up_weight,
        down_weight,
    )
    kv_sems = [dma((KV - 1,))] * 2
    tp_sems = [dma((TP - 1,))] * 2
    return pl.pallas_call(
        functools.partial(kernel, KV, TP),
        out_shape=jax.ShapeDtypeStruct((rows, piece), residual.dtype),
        in_specs=[any_spec] * len(args),
        out_specs=pl.BlockSpec(memory_space=pltpu.VMEM),
        scratch_shapes=[
            pltpu.VMEM((rows, piece), BF16),
            pltpu.VMEM(keys.shape, BF16),
            pltpu.VMEM(values.shape, BF16),
            pltpu.VMEM((width // LANES, LANES), BF16),
            pltpu.VMEM((width, qcols + 2 * LANES), BF16),
            pltpu.VMEM((1, head_lambda.shape[0]), F32),
            pltpu.VMEM((1, head_gain.shape[0]), BF16),
            pltpu.VMEM(out_weight.shape, BF16),
            pltpu.VMEM((width // LANES, LANES), BF16),
            pltpu.VMEM(up_weight.shape, BF16),
            pltpu.VMEM(down_weight.shape, BF16),
            pltpu.VMEM((TP, rows, LANES), BF16),
            pltpu.VMEM((KV, rows, qcols), BF16),
            pltpu.VMEM((KV, 1, 3 * LANES), F32),
            pltpu.VMEM((KV, 1, 3 * LANES), F32),
            pltpu.VMEM((KV, lines, LANES), BF16),
            pltpu.VMEM((KV, 1, LANES), F32),
            pltpu.VMEM((TP, rows, width), F32),
            pltpu.VMEM((KV, 1, LANES), F32),
            pltpu.VMEM((KV, rows, share), F32),
            pltpu.VMEM((KV, rows, share), F32),
            pltpu.VMEM((KV, rows, share), BF16),
            pltpu.VMEM((width // LANES, rows, LANES), F32),
            pltpu.VMEM((TP, rows, LANES), F32),
            dma((13,)),
            *tp_sems,
            *kv_sems,
            *kv_sems,
            *kv_sems,
            *kv_sems,
            *tp_sems,
            *kv_sems,
            *kv_sems,
            *kv_sems,
            *tp_sems,
        ],
        compiler_params=pltpu.CompilerParams(
            collective_id=0, has_side_effects=True, vmem_limit_bytes=48 * 1024 * 1024
        ),
        name="layer",
    )(*args)


def solution(mesh):
    in_specs = (
        P("grp", ("kv", "tp")),
        P("grp", "kv", "tp", None),
        P("grp", "kv", "tp", None),
        P("kv"),
        P("kv", "tp"),
        P("kv", "tp"),
        P("kv", "tp"),
        P("tp"),
        P(),
        P("tp", "kv"),
        P("kv"),
        P("kv", "tp"),
        P("tp", "kv"),
    )
    out_specs = P("grp", ("kv", "tp"))
    fn = functools.partial(body, mesh.shape["kv"], mesh.shape["tp"])
    return jax.shard_map(fn, mesh=mesh, in_specs=in_specs, out_specs=out_specs, check_vma=False)
```

time: 214 us -> 101 us (0.47)
  Pallas kernels: 0 us -> 90.7 us
  waiting for transfers between devices: 81.5 us -> 0 us
  starting transfers between devices: 63.1 us -> 0 us
  blocking collectives: 23.9 us -> 0 us
  local copies, waits for them, and re-layouts: 27.8 us -> 9.83 us
  matrix products: 10.2 us -> 0 us
  other arithmetic: 5.41 us -> 0 us
    pallas_call x0 -> x1, Pallas kernels: none -> 90.7 us  [body(): pl.pallas_call(functools.partial(kernel, KV, TP), out_shape=jax.ShapeDtyp...]
    all_to_all x7 -> x0, waiting for transfers between devices: 81.5 us -> none  [the longest x6 70 us: sent_to_all(): lax.all_to_all(jnp.broadcast_to(shard[None], (devices, *shard.shape)), ax...]
    all_to_all x7 -> x0, starting transfers between devices: 63.1 us -> none  [the longest x6 59.1 us: sent_to_all(): lax.all_to_all(jnp.broadcast_to(shard[None], (devices, *shard.shape)), ax...]
    all_to_all x2 -> x0, blocking collectives: 23.9 us -> none  [sum_at_owner(): lax.all_to_all(cut_along(shard, dim, devices), axis, 0, 0, tiled=True)]
    slice x17 -> x0, local copies, waits for them, and re-layouts: 10.5 us -> none  [the longest x10 10.4 us: joined_by_halves(): part[side::2]]
    dot_general x9 -> x0, matrix products: 10.2 us -> none  [the longest x1 3.03 us: body(): jnp.einsum('bkgcp,bpkv->bkgcv', expo.astype(bf16), cache_values, preferre...]
    broadcast_in_dim x6 -> x0, local copies, waits for them, and re-layouts: 3.89 us -> none  [sent_to_all(): jnp.broadcast_to(shard[None], (devices, *shard.shape))]
    unnamed x35 -> x23, local copies, waits for them, and re-layouts: 10 us -> 9.83 us
  transfers between devices with their start and end apart: 7 -> 0, of which waited for: 7 -> 0; matrix products, arithmetic and copies ran while one was open for 5% -> 0% of each run, Pallas kernels for 0% -> 0%
where the time goes in v1:
time: 101 us
  Pallas kernels  90.7 us (90%)
  local copies, waits for them, and re-layouts  9.83 us (10%)
    pallas_call x1, Pallas kernels, body(): pl.pallas_call(functools.partial(kernel, KV, TP), out_shape=jax.ShapeDtyp...  90.7 us
    unnamed x23, local copies, waits for them, and re-layouts  9.83 us

profile of v1, /device:TPU:33, one launch (start us, length us, event | category | flops | bytes accessed | tf_op | source)
XLA Modules:
  0.0 100.5 jit_solution(12280791182888303969)
XLA Ops:
  0.0 0.0 copy-start
  0.0 1.2 %copy-done = bf16[256,2048]{1,0:T(8,128)(2,1)S(1)} copy-done((bf16[256,2048]{1,0:T(8,128)(2,1)S(1)}, bf16[256,2048]{1,0:T(8,128)(2,1)}, u32[]{:S(2)}) %copy-start) | copy-done | bytes 1048600
  1.2 0.0 copy-start.1
  1.2 1.2 %copy-done.1 = bf16[2048,256]{1,0:T(8,128)(2,1)S(1)} copy-done((bf16[2048,256]{1,0:T(8,128)(2,1)S(1)}, bf16[2048,256]{1,0:T(8,128)(2,1)}, u32[]{:S(2)}) %copy-start.1) | copy-done | bytes 1048600
  2.5 0.0 copy-start.2
  2.5 0.9 copy-done.2
  3.4 0.0 copy-start.3
  3.4 0.9 copy-done.3
  4.3 0.0 copy-start.4
  4.3 0.8 copy-done.4
  5.1 0.0 copy-start.5
  5.1 0.8 copy-done.5
  5.9 0.0 copy-start.6
  5.9 0.7 copy-done.6
  6.6 0.0 copy-start.7
  6.6 0.7 copy-done.7
  7.3 0.0 copy-start.8
  7.3 0.7 copy-done.8
  7.9 0.0 copy-start.9
  7.9 0.7 copy-done.9
  8.6 0.0 copy-start.10
  8.6 0.7 copy-done.10
  9.3 90.7 %layer.1 = bf16[16,32]{1,0:T(8,128)(2,1)S(1)} custom-call(bf16[16,32]{1,0:T(8,128)(2,1)S(1)} %copy-done.6, bf16[16,1024,128]{2,1,0:T(8,128)(2,1)} %bitcast.10, bf16[16,1024,128]{2,1,0:T(8,128)(2,1)} %bitcast.11, bf16[2,128]{1,0:T(2,128)(2,1)S(1)} %bitcast.6, bf16[256,256]{1,0:T(8,128)(2,1)S(1)} %copy-done.2, bf16[256,128]{1,0:T(8,128)(2,1)S(1)} %copy-done.4, ...), custom_call_target="tpu_custom_call" | custom-call | tf_op jit(solution)/shard_map/layer/pallas_call | solution.py:405
  99.9 0.6 copy.15
Async XLA Ops:
  0.0 1.2 %copy-start = (bf16[256,2048]{1,0:T(8,128)(2,1)S(1)}, bf16[256,2048]{1,0:T(8,128)(2,1)}, u32[]{:S(2)}) copy-start(bf16[256,2048]{1,0:T(8,128)(2,1)} %wu_h.1) | copy-start | bytes 3145732
  1.2 1.2 %copy-start.1 = (bf16[2048,256]{1,0:T(8,128)(2,1)S(1)}, bf16[2048,256]{1,0:T(8,128)(2,1)}, u32[]{:S(2)}) copy-start(bf16[2048,256]{1,0:T(8,128)(2,1)} %wd_h.1) | copy-start | bytes 3145732
  2.5 0.9 copy-start.2
  3.4 0.9 copy-start.3
  4.3 0.8 copy-start.4
  5.1 0.8 copy-start.5
  5.9 0.7 copy-start.6
  6.6 0.7 copy-start.7
  7.3 0.7 copy-start.8
  7.9 0.7 copy-start.9
  8.6 0.7 copy-start.10

commit v2 on v1

--- a/solution.py
+++ b/solution.py
@@ -76,8 +76,11 @@
     qbuf,
     kvs,
     kvr,
+    wsend,
     wbuf,
+    mlsend,
     mlbuf,
+    nbuf,
     dbuf,
     sqbuf,
     us,
@@ -85,6 +88,7 @@
     hbuf,
     fs,
     fr,
+    ring_sem,
     load_sem,
     a_send,
     a_recv,
@@ -96,6 +100,8 @@
     w_recv,
     m_send,
     m_recv,
+    n_send,
+    n_recv,
     d_send,
     d_recv,
     s_send,
@@ -126,16 +132,17 @@
         return copy
 
     ld_res = load(res_h, res, 0)
+    barrier = pltpu.get_barrier_semaphore()
     for u in range(1, TP):
         peer = lax.rem(t + u, TP)
-        pl.semaphore_signal(
-            pltpu.get_barrier_semaphore(), inc=1, device_id={"tp": peer}, device_id_type=MESH
-        )
-    for u in far_first(KV):
-        peer = lax.rem(z + u, KV)
-        pl.semaphore_signal(
-            pltpu.get_barrier_semaphore(), inc=1, device_id={"kv": peer}, device_id_type=MESH
-        )
+        pl.semaphore_signal(barrier, inc=1, device_id={"tp": peer}, device_id_type=MESH)
+
+    def both_ways(sem, d):
+        for u in (d, KV - d):
+            peer = lax.rem(z + u, KV)
+            pl.semaphore_signal(sem, inc=1, device_id={"kv": peer}, device_id_type=MESH)
+
+    both_ways(barrier, 1)
     ld_ng = load(ng_h, ng, 1)
     ld_wq = load(wq_h, wp.at[:, 0:qcols], 2)
     ld_wk = load(wk_h, wp.at[:, qcols : qcols + LANES], 3)
@@ -167,12 +174,14 @@
     kv_order = far_first(KV)
     tp_order = far_first(TP)
 
-    def spread(src_of, dst, sems, rsems, axis):
-        me, n, order = (z, KV, kv_order) if axis == "kv" else (t, TP, tp_order)
+    def spread(src_of, dst, sems, rsems, axis, order=None):
+        me, n = (z, KV) if axis == "kv" else (t, TP)
+        if order is None:
+            order = kv_order if axis == "kv" else tp_order
         copies = []
         for d in order:
             peer = lax.rem(me + d, n)
-            copies.append(send(src_of(peer), dst.at[me], sems.at[d - 1], rsems.at[d - 1], axis, peer))
+            copies.append(send(src_of(peer), dst, sems.at[d - 1], rsems.at[d - 1], axis, peer))
         return copies
 
     def arrive(copies):
@@ -184,8 +193,14 @@
     tiled = jnp.concatenate([own_piece] * per_tile, axis=1)
     at = iota(tiled.shape, 1) // piece == lax.rem(t, per_tile)
     abuf[t] = jnp.where(at, tiled, 0.0).astype(BF16)
-    pl.semaphore_wait(pltpu.get_barrier_semaphore(), TP - 1 + KV - 1)
-    arrive(spread(lambda peer: abuf.at[t], abuf, a_send, a_recv, "tp"))
+    pl.semaphore_wait(barrier, TP - 1 + 2)
+    a_copies = spread(lambda peer: abuf.at[t], abuf.at[t], a_send, a_recv, "tp")
+    both_ways(ring_sem.at[0], 1)
+    pl.semaphore_wait(ring_sem.at[0], 2)
+    both_ways(ring_sem.at[1], 2)
+    arrive(a_copies)
+    pl.semaphore_wait(ring_sem.at[1], 2)
+    both_ways(ring_sem.at[2], 4)
     block = jnp.concatenate(
         [
             sum(abuf[k * per_tile + j].astype(F32) for j in range(per_tile))
@@ -205,8 +220,9 @@
     for j in range(KV):
         kvs[j] = jnp.concatenate([proj[j : j + 1, qcols:], square], axis=1)
     kvr[z] = kvs[z]
-    q_copies = spread(lambda peer: qbuf.at[z], qbuf, q_send, q_recv, "kv")
-    r_copies = spread(lambda peer: kvs.at[peer], kvr, r_send, r_recv, "kv")
+    pl.semaphore_wait(ring_sem.at[2], 2)
+    q_copies = spread(lambda peer: qbuf.at[z], qbuf.at[z], q_send, q_recv, "kv")
+    r_copies = spread(lambda peer: kvs.at[peer], kvr.at[z], r_send, r_recv, "kv")
     arrive(q_copies)
     arrive(r_copies)
     q_sum = qbuf[0].astype(F32)
@@ -272,36 +288,46 @@
     own_part = jnp.exp(own - new_top)
     total = total * old_part + own_part
     weighted = weighted * old_part + own_part * new_value
-    wbuf[z] = weighted.astype(BF16)
-    lane = iota((lines, LANES), 1)
-    both = jnp.where(lane == line, new_top, jnp.where(lane == line + half, total, 0.0))
-    mlbuf[z] = jnp.sum(both, axis=0, keepdims=True)
-    m_copies = spread(lambda peer: mlbuf.at[z], mlbuf, m_send, m_recv, "kv")
-    w_copies = spread(lambda peer: wbuf.at[z], wbuf, w_send, w_recv, "kv")
+    quarter = lines // 4
+    mine = lax.rem(z, 4)
+    lane = iota((quarter, LANES), 1)
+    line = iota((quarter, LANES), 0)
+    for c in range(4):
+        at = slice(c * quarter, (c + 1) * quarter)
+        wsend[c] = weighted[at].astype(BF16)
+        both = jnp.where(lane == line, new_top[at], jnp.where(lane == line + half, total[at], 0.0))
+        mlsend[c] = jnp.sum(both, axis=0, keepdims=True)
+    wbuf[z] = wsend[mine]
+    mlbuf[z] = mlsend[mine]
+    m_copies = spread(lambda peer: mlsend.at[lax.rem(peer, 4)], mlbuf.at[z], m_send, m_recv, "kv")
+    w_copies = spread(lambda peer: wsend.at[lax.rem(peer, 4)], wbuf.at[z], w_send, w_recv, "kv")
     arrive(m_copies)
     ml = jnp.concatenate([mlbuf[j] for j in range(KV)], axis=0)
     shares = jnp.exp(ml - jnp.max(ml, axis=0, keepdims=True))
     grand = jnp.sum(shares * pltpu.roll(ml, half, 1), axis=0, keepdims=True)
-    in_use = iota(ml.shape, 1) < half
+    in_use = iota(ml.shape, 1) < quarter
     shares = jnp.where(in_use, shares / jnp.where(in_use[0:1], grand, 1.0), 0.0)
     columns = jnp.transpose(shares)
     arrive(w_copies)
-    attended = columns[0:lines, 0:1] * wbuf[0].astype(F32)
+    attended = columns[0:quarter, 0:1] * wbuf[0].astype(F32)
     for j in range(1, KV):
-        attended = attended + columns[0:lines, j : j + 1] * wbuf[j].astype(F32)
+        attended = attended + columns[0:quarter, j : j + 1] * wbuf[j].astype(F32)
     ld_lam.wait()
     ld_hg.wait()
     lambdas = lam[0:1, 0:1]
     for g in range(1, heads):
         lambdas = jnp.where(
-            lax.rem(iota((lines, 1), 0), maps) // 2 == g, lam[0:1, g : g + 1], lambdas
+            lax.rem(iota((quarter, 1), 0), maps) // 2 == g, lam[0:1, g : g + 1], lambdas
         )
-    diff = attended - lambdas * pltpu.roll(attended, lines - 1, 0)
+    diff = attended - lambdas * pltpu.roll(attended, quarter - 1, 0)
     normed = (
         diff
         * lax.rsqrt(jnp.mean(diff * diff, axis=1, keepdims=True) + EPS)
         * hg[...].astype(F32)
     ).astype(BF16)
+    nbuf[mine] = normed
+    arrive(spread(lambda peer: nbuf.at[mine], nbuf.at[mine], n_send, n_recv, "kv", (2, 1, KV - 1)))
+    normed = jnp.concatenate([nbuf[c] for c in range(4)], axis=0)
     outs = []
     for g in range(heads):
         pick = iota((rows, lines), 1) == iota((rows, lines), 0) * maps + 2 * g
@@ -309,23 +335,25 @@
     heads_out = jnp.concatenate(outs, axis=1).astype(BF16)
     ld_wo.wait()
     dbuf[t] = dot(heads_out, wo[...])
-    arrive(spread(lambda peer: dbuf.at[t], dbuf, d_send, d_recv, "tp"))
+    arrive(spread(lambda peer: dbuf.at[t], dbuf.at[t], d_send, d_recv, "tp"))
     projected = dbuf[0]
     for j in range(1, TP):
         projected = projected + dbuf[j]
     mixed = (block + projected).astype(BF16).astype(F32)
     sqbuf[z] = to_lanes(jnp.sum(mixed * mixed, axis=1, keepdims=True))
-    s_copies = spread(lambda peer: sqbuf.at[z], sqbuf, s_send, s_recv, "kv")
+    s_copies = spread(lambda peer: sqbuf.at[z], sqbuf.at[z], s_send, s_recv, "kv")
     ld_mg.wait()
     gain2 = jnp.concatenate([mg[k : k + 1, :] for k in range(width // LANES)], axis=1).astype(F32)
     scaled2 = (mixed * gain2).astype(BF16)
     ld_wu.wait()
     up = dot(scaled2, wu[...])
-    share_width = up.shape[1] // KV
-    for j in range(KV):
-        us[j] = up[:, j * share_width : (j + 1) * share_width].astype(us.dtype)
-    ur[z] = us[z]
-    u_copies = spread(lambda peer: us.at[peer], ur, u_send, u_recv, "kv")
+    owners = KV // 2
+    owned = lax.rem(z, owners)
+    share_width = up.shape[1] // owners
+    for j in range(owners):
+        us[j] = up[:, j * share_width : (j + 1) * share_width].astype(BF16)
+    ur[z] = us[owned]
+    u_copies = spread(lambda peer: us.at[lax.rem(peer, owners)], ur.at[z], u_send, u_recv, "kv")
     arrive(s_copies)
     square2 = sqbuf[0]
     for j in range(1, KV):
@@ -336,15 +364,22 @@
     for j in range(1, KV):
         up_sum = up_sum + ur[j].astype(F32)
     act = jnp.maximum(inv2 * up_sum, 0.0)
-    hbuf[z] = (act * act).astype(BF16)
-    arrive(spread(lambda peer: hbuf.at[z], hbuf, h_send, h_recv, "kv"))
-    hidden = jnp.concatenate([hbuf[j] for j in range(KV)], axis=1)
+    hbuf[owned] = (act * act).astype(BF16)
+    near = [owners // 2]
+    for d in range(owners // 2 - 1, 0, -1):
+        near += [d, KV - d]
+    arrive(spread(lambda peer: hbuf.at[owned], hbuf.at[owned], h_send, h_recv, "kv", near))
+    hidden = jnp.concatenate([hbuf[j] for j in range(owners)], axis=1)
     ld_wd.wait()
     down = dot(hidden, wd[...])
     for k in range(width // LANES):
         fs[k] = down[:, k * LANES : (k + 1) * LANES]
     fr[t] = fs[t // per_tile]
-    arrive(spread(lambda peer: fs.at[peer // per_tile], fr, f_send, f_recv, "tp"))
+    earlier = len(started)
+    f_copies = spread(lambda peer: fs.at[peer // per_tile], fr.at[t], f_send, f_recv, "tp")
+    for copy in started[:earlier]:
+        copy.wait_send()
+    arrive(f_copies)
     y = fr[0]
     for j in range(1, TP):
         y = y + fr[j]
@@ -354,7 +389,7 @@
     for k in range(1, per_tile):
         result = jnp.where(lax.rem(t, per_tile) == k, y[:, k * piece : (k + 1) * piece], result)
     out_ref[...] = result.astype(out_ref.dtype)
-    for copy in started:
+    for copy in f_copies:
         copy.wait_send()
 
 
@@ -380,7 +415,7 @@
     width = out_weight.shape[1]
     qcols = query_weight.shape[1]
     lines = rows * qcols * 2 // LANES
-    share = up_weight.shape[1] // KV
+    share = up_weight.shape[1] * 2 // KV
     any_spec = pl.BlockSpec(memory_space=pl.ANY)
     dma = pltpu.SemaphoreType.DMA
     keys = cache_keys.reshape(rows, positions, depth)
@@ -423,17 +458,22 @@
             pltpu.VMEM((KV, rows, qcols), BF16),
             pltpu.VMEM((KV, 1, 3 * LANES), F32),
             pltpu.VMEM((KV, 1, 3 * LANES), F32),
-            pltpu.VMEM((KV, lines, LANES), BF16),
+            pltpu.VMEM((4, lines // 4, LANES), BF16),
+            pltpu.VMEM((KV, lines // 4, LANES), BF16),
+            pltpu.VMEM((4, 1, LANES), F32),
             pltpu.VMEM((KV, 1, LANES), F32),
+            pltpu.VMEM((4, lines // 4, LANES), BF16),
             pltpu.VMEM((TP, rows, width), F32),
             pltpu.VMEM((KV, 1, LANES), F32),
-            pltpu.VMEM((KV, rows, share), F32),
-            pltpu.VMEM((KV, rows, share), F32),
+            pltpu.VMEM((KV // 2, rows, share), BF16),
             pltpu.VMEM((KV, rows, share), BF16),
+            pltpu.VMEM((KV // 2, rows, share), BF16),
             pltpu.VMEM((width // LANES, rows, LANES), F32),
             pltpu.VMEM((TP, rows, LANES), F32),
+            pltpu.SemaphoreType.REGULAR((3,)),
             dma((13,)),
             *tp_sems,
+            *kv_sems,
             *kv_sems,
             *kv_sems,
             *kv_sems,
@@ -445,7 +485,7 @@
             *tp_sems,
         ],
         compiler_params=pltpu.CompilerParams(
-            collective_id=0, has_side_effects=True, vmem_limit_bytes=48 * 1024 * 1024
+            collective_id=0, has_side_effects=True, vmem_limit_bytes=64 * 1000 * 1000
         ),
         name="layer",
     )(*args)

time: 101 us -> 84.7 us (0.84)
  local copies, waits for them, and re-layouts: 9.83 us -> 1.28 us
  Pallas kernels: 90.7 us -> 83.2 us
    unnamed x23 -> x1, local copies, waits for them, and re-layouts: 9.83 us -> 1.28 us
    pallas_call x1, Pallas kernels: 90.7 us -> 83.2 us  [body(): pl.pallas_call(functools.partial(kernel, KV, TP), out_shape=jax.ShapeDtyp...]
where the time goes in v2:
time: 84.7 us; the launch traced here: 84.5 us
  Pallas kernels  83.2 us (98%)
  local copies, waits for them, and re-layouts  1.28 us (2%)
    pallas_call x1, Pallas kernels, body(): pl.pallas_call(functools.partial(kernel, KV, TP), out_shape=jax.ShapeDtyp...  83.2 us

profile of v2, /device:TPU:33, one launch (start us, length us, event | category | flops | bytes accessed | tf_op | source)
XLA Modules:
  0.0 84.5 jit_solution(15579251751701454607)
XLA Ops:
  0.0 83.2 %layer.1 = bf16[16,32]{1,0:T(8,128)(2,1)} custom-call(bf16[16,32]{1,0:T(8,128)(2,1)} %res_h.1, bf16[16,1024,128]{2,1,0:T(8,128)(2,1)} %bitcast.6, bf16[16,1024,128]{2,1,0:T(8,128)(2,1)} %bitcast.7, bf16[2,128]{1,0:T(2,128)(2,1)} %bitcast.8, bf16[256,256]{1,0:T(8,128)(2,1)} %wq_h.1, bf16[256,128]{1,0:T(8,128)(2,1)} %wk_h.1, bf16[256,128]{1,0:T(8,128)(2,1)} %wv_h.1, ...), custom_call_target="tpu_custom_call" | custom-call | tf_op jit(solution)/shard_map/layer/pallas_call | solution.py:440
  83.3 1.3 %copy.15 = bf16[16,32]{1,0:T(8,128)(2,1)} copy(bf16[16,32]{1,0:T(8,128)(2,1)} %layer.1) | data formatting | bytes 2048

commit v3 on v2

--- a/solution.py
+++ b/solution.py
@@ -76,6 +76,7 @@
     qbuf,
     kvs,
     kvr,
+    lined_s,
     wsend,
     wbuf,
     mlsend,
@@ -143,18 +144,11 @@
             pl.semaphore_signal(sem, inc=1, device_id={"kv": peer}, device_id_type=MESH)
 
     both_ways(barrier, 1)
+    both_ways(barrier, 2)
     ld_ng = load(ng_h, ng, 1)
     ld_wq = load(wq_h, wp.at[:, 0:qcols], 2)
     ld_wk = load(wk_h, wp.at[:, qcols : qcols + LANES], 3)
     ld_wv = load(wv_h, wp.at[:, qcols + LANES : qcols + 2 * LANES], 4)
-    ld_keys = load(keys_h, keys, 5)
-    ld_values = load(values_h, values, 6)
-    ld_lam = load(lam_h, lam, 7)
-    ld_hg = load(hg_h, hg, 8)
-    ld_wo = load(wo_h, wo, 9)
-    ld_mg = load(mg_h, mg, 10)
-    ld_wu = load(wu_h, wu, 11)
-    ld_wd = load(wd_h, wd, 12)
 
     started = []
 
@@ -193,14 +187,12 @@
     tiled = jnp.concatenate([own_piece] * per_tile, axis=1)
     at = iota(tiled.shape, 1) // piece == lax.rem(t, per_tile)
     abuf[t] = jnp.where(at, tiled, 0.0).astype(BF16)
-    pl.semaphore_wait(barrier, TP - 1 + 2)
+    pl.semaphore_wait(barrier, TP - 1 + 4)
     a_copies = spread(lambda peer: abuf.at[t], abuf.at[t], a_send, a_recv, "tp")
-    both_ways(ring_sem.at[0], 1)
+    both_ways(ring_sem.at[0], 2)
     pl.semaphore_wait(ring_sem.at[0], 2)
-    both_ways(ring_sem.at[1], 2)
+    both_ways(ring_sem.at[1], 4)
     arrive(a_copies)
-    pl.semaphore_wait(ring_sem.at[1], 2)
-    both_ways(ring_sem.at[2], 4)
     block = jnp.concatenate(
         [
             sum(abuf[k * per_tile + j].astype(F32) for j in range(per_tile))
@@ -220,9 +212,17 @@
     for j in range(KV):
         kvs[j] = jnp.concatenate([proj[j : j + 1, qcols:], square], axis=1)
     kvr[z] = kvs[z]
-    pl.semaphore_wait(ring_sem.at[2], 2)
+    pl.semaphore_wait(ring_sem.at[1], 2)
     q_copies = spread(lambda peer: qbuf.at[z], qbuf.at[z], q_send, q_recv, "kv")
     r_copies = spread(lambda peer: kvs.at[peer], kvr.at[z], r_send, r_recv, "kv")
+    ld_keys = load(keys_h, keys, 5)
+    ld_values = load(values_h, values, 6)
+    ld_lam = load(lam_h, lam, 7)
+    ld_hg = load(hg_h, hg, 8)
+    ld_wo = load(wo_h, wo, 9)
+    ld_mg = load(mg_h, mg, 10)
+    ld_wu = load(wu_h, wu, 11)
+    ld_wd = load(wd_h, wd, 12)
     arrive(q_copies)
     arrive(r_copies)
     q_sum = qbuf[0].astype(F32)
@@ -238,16 +238,12 @@
     new_value = (inv_own * r_sum[:, LANES : 2 * LANES]).astype(BF16).astype(F32)
     query = (to_rows(inv_lanes, rows) * q_sum).astype(BF16)
 
-    pick = (iota((lines, rows), 0) // maps == iota((lines, rows), 1)).astype(BF16)
-    spreadq = dot(pick, query)
-    line = iota((lines, LANES), 0)
-    chosen = spreadq[:, 0:LANES]
-    for g in range(1, heads):
-        chosen = jnp.where(
-            lax.rem(line, maps) // 2 == g, spreadq[:, g * LANES : (g + 1) * LANES], chosen
-        )
-    mine = iota((lines, LANES), 1) // half == lax.rem(line, 2)
-    lined = jnp.where(mine, chosen, 0.0) * (1.0 / half**0.5)
+    lane = iota((rows, LANES), 1)
+    for g in range(heads):
+        head = query[:, g * LANES : (g + 1) * LANES].astype(F32) * (1.0 / half**0.5)
+        for c in range(2):
+            lined_s[pl.ds(2 * g + c, rows, stride=maps), :] = jnp.where(lane // half == c, head, 0.0)
+    lined = lined_s[...]
 
     ld_keys.wait()
     ld_values.wait()
@@ -327,11 +323,9 @@
     ).astype(BF16)
     nbuf[mine] = normed
     arrive(spread(lambda peer: nbuf.at[mine], nbuf.at[mine], n_send, n_recv, "kv", (2, 1, KV - 1)))
-    normed = jnp.concatenate([nbuf[c] for c in range(4)], axis=0)
-    outs = []
-    for g in range(heads):
-        pick = iota((rows, lines), 1) == iota((rows, lines), 0) * maps + 2 * g
-        outs.append(dot(pick.astype(BF16), normed))
+    for c in range(4):
+        lined_s[c * quarter : (c + 1) * quarter, :] = nbuf[c].astype(F32)
+    outs = [lined_s[pl.ds(2 * g, rows, stride=maps), :] for g in range(heads)]
     heads_out = jnp.concatenate(outs, axis=1).astype(BF16)
     ld_wo.wait()
     dbuf[t] = dot(heads_out, wo[...])
@@ -458,6 +452,7 @@
             pltpu.VMEM((KV, rows, qcols), BF16),
             pltpu.VMEM((KV, 1, 3 * LANES), F32),
             pltpu.VMEM((KV, 1, 3 * LANES), F32),
+            pltpu.VMEM((lines, LANES), F32),
             pltpu.VMEM((4, lines // 4, LANES), BF16),
             pltpu.VMEM((KV, lines // 4, LANES), BF16),
             pltpu.VMEM((4, 1, LANES), F32),
@@ -470,7 +465,7 @@
             pltpu.VMEM((KV // 2, rows, share), BF16),
             pltpu.VMEM((width // LANES, rows, LANES), F32),
             pltpu.VMEM((TP, rows, LANES), F32),
-            pltpu.SemaphoreType.REGULAR((3,)),
+            pltpu.SemaphoreType.REGULAR((2,)),
             dma((13,)),
             *tp_sems,
             *kv_sems,

time: 84.7 us -> 83.2 us (0.982)
  Pallas kernels: 83.2 us -> 81.8 us
    pallas_call x1, Pallas kernels: 83.2 us -> 81.8 us  [body(): pl.pallas_call(functools.partial(kernel, KV, TP), out_shape=jax.ShapeDtyp...]
where the time goes in v3:
time: 83.2 us; the launch traced here: 83.1 us
  Pallas kernels  81.8 us (98%)
  local copies, waits for them, and re-layouts  1.28 us (2%)
    pallas_call x1, Pallas kernels, body(): pl.pallas_call(functools.partial(kernel, KV, TP), out_shape=jax.ShapeDtyp...  81.8 us

profile of v3, /device:TPU:33, one launch (start us, length us, event | category | flops | bytes accessed | tf_op | source)
XLA Modules:
  0.0 83.1 jit_solution(17941045221310846158)
XLA Ops:
  0.0 81.8 %layer.1 = bf16[16,32]{1,0:T(8,128)(2,1)} custom-call(bf16[16,32]{1,0:T(8,128)(2,1)} %res_h.1, bf16[16,1024,128]{2,1,0:T(8,128)(2,1)} %bitcast.6, bf16[16,1024,128]{2,1,0:T(8,128)(2,1)} %bitcast.7, bf16[2,128]{1,0:T(2,128)(2,1)} %bitcast.8, bf16[256,256]{1,0:T(8,128)(2,1)} %wq_h.1, bf16[256,128]{1,0:T(8,128)(2,1)} %wk_h.1, bf16[256,128]{1,0:T(8,128)(2,1)} %wv_h.1, ...), custom_call_target="tpu_custom_call" | custom-call | tf_op jit(solution)/shard_map/layer/pallas_call | solution.py:434
  81.8 1.3 %copy.15 = bf16[16,32]{1,0:T(8,128)(2,1)} copy(bf16[16,32]{1,0:T(8,128)(2,1)} %layer.1) | data formatting | bytes 2048

commit v4 on v3

--- a/solution.py
+++ b/solution.py
@@ -16,12 +16,41 @@
 
 
 def far_first(n):
-    order = [n // 2]
-    for k in range(1, n // 2 + 1):
-        for d in (n // 2 - k, n // 2 + k):
-            if 0 < d < n:
-                order.append(d)
-    return order
+    def distance(k):
+        odd = lax.rem(k, 2)
+        return n // 2 + odd * ((k + 1) // 2) - (1 - odd) * (k // 2)
+
+    return distance
+
+
+def loop(n, step):
+    def run(k, carry):
+        step(k)
+        return carry
+
+    lax.fori_loop(0, n, run, 0)
+
+
+class Spread:
+    def __init__(self, copy_to, distances, steps):
+        self.copy_to, self.distances, self.steps = copy_to, distances, steps
+
+    def each(self, act):
+        if self.steps is None:
+            for d in self.distances:
+                act(self.copy_to(d))
+        else:
+            loop(self.steps, lambda k: act(self.copy_to(self.distances(k))))
+
+    def start(self):
+        self.each(lambda copy: copy.start())
+        return self
+
+    def arrive(self):
+        self.each(lambda copy: copy.wait_recv())
+
+    def sent(self):
+        self.each(lambda copy: copy.wait_send())
 
 
 def iota(shape, dim):
@@ -134,9 +163,11 @@
 
     ld_res = load(res_h, res, 0)
     barrier = pltpu.get_barrier_semaphore()
-    for u in range(1, TP):
-        peer = lax.rem(t + u, TP)
+    def greet(k):
+        peer = lax.rem(t + k + 1, TP)
         pl.semaphore_signal(barrier, inc=1, device_id={"tp": peer}, device_id_type=MESH)
+
+    loop(TP - 1, greet)
 
     def both_ways(sem, d):
         for u in (d, KV - d):
@@ -152,35 +183,34 @@
 
     started = []
 
-    def send(src, dst, ssem, rsem, axis, peer):
-        copy = pltpu.make_async_remote_copy(
-            src_ref=src,
-            dst_ref=dst,
-            send_sem=ssem,
-            recv_sem=rsem,
-            device_id={axis: peer},
-            device_id_type=MESH,
-        )
-        copy.start()
-        started.append(copy)
-        return copy
-
-    kv_order = far_first(KV)
-    tp_order = far_first(TP)
-
-    def spread(src_of, dst, sems, rsems, axis, order=None):
+    def spread(src_of, dst, ssem, rsem, axis, distances=None):
         me, n = (z, KV) if axis == "kv" else (t, TP)
-        if order is None:
-            order = kv_order if axis == "kv" else tp_order
-        copies = []
-        for d in order:
+
+        def copy_to(d):
             peer = lax.rem(me + d, n)
-            copies.append(send(src_of(peer), dst, sems.at[d - 1], rsems.at[d - 1], axis, peer))
-        return copies
-
-    def arrive(copies):
-        for copy in copies:
-            copy.wait_recv()
+            return pltpu.make_async_remote_copy(
+                src_ref=src_of(peer),
+                dst_ref=dst,
+                send_sem=ssem.at[d - 1],
+                recv_sem=rsem.at[d - 1],
+                device_id={axis: peer},
+                device_id_type=MESH,
+            )
+
+        if distances is None:
+            out = Spread(copy_to, far_first(n), n - 1)
+        else:
+            out = Spread(copy_to, distances, None)
+        started.append(out)
+        return out
+
+    def start_both(first, second):
+        def step(k):
+            d = first.distances(k)
+            first.copy_to(d).start()
+            second.copy_to(d).start()
+
+        loop(first.steps, step)
 
     ld_res.wait()
     own_piece = res[...].astype(F32)
@@ -188,11 +218,11 @@
     at = iota(tiled.shape, 1) // piece == lax.rem(t, per_tile)
     abuf[t] = jnp.where(at, tiled, 0.0).astype(BF16)
     pl.semaphore_wait(barrier, TP - 1 + 4)
-    a_copies = spread(lambda peer: abuf.at[t], abuf.at[t], a_send, a_recv, "tp")
+    a_copies = spread(lambda peer: abuf.at[t], abuf.at[t], a_send, a_recv, "tp").start()
     both_ways(ring_sem.at[0], 2)
     pl.semaphore_wait(ring_sem.at[0], 2)
     both_ways(ring_sem.at[1], 4)
-    arrive(a_copies)
+    a_copies.arrive()
     block = jnp.concatenate(
         [
             sum(abuf[k * per_tile + j].astype(F32) for j in range(per_tile))
@@ -215,6 +245,8 @@
     pl.semaphore_wait(ring_sem.at[1], 2)
     q_copies = spread(lambda peer: qbuf.at[z], qbuf.at[z], q_send, q_recv, "kv")
     r_copies = spread(lambda peer: kvs.at[peer], kvr.at[z], r_send, r_recv, "kv")
+
+    start_both(r_copies, q_copies)
     ld_keys = load(keys_h, keys, 5)
     ld_values = load(values_h, values, 6)
     ld_lam = load(lam_h, lam, 7)
@@ -223,8 +255,8 @@
     ld_mg = load(mg_h, mg, 10)
     ld_wu = load(wu_h, wu, 11)
     ld_wd = load(wd_h, wd, 12)
-    arrive(q_copies)
-    arrive(r_copies)
+    q_copies.arrive()
+    r_copies.arrive()
     q_sum = qbuf[0].astype(F32)
     r_sum = kvr[0]
     for j in range(1, KV):
@@ -297,14 +329,15 @@
     mlbuf[z] = mlsend[mine]
     m_copies = spread(lambda peer: mlsend.at[lax.rem(peer, 4)], mlbuf.at[z], m_send, m_recv, "kv")
     w_copies = spread(lambda peer: wsend.at[lax.rem(peer, 4)], wbuf.at[z], w_send, w_recv, "kv")
-    arrive(m_copies)
+    start_both(m_copies, w_copies)
+    m_copies.arrive()
     ml = jnp.concatenate([mlbuf[j] for j in range(KV)], axis=0)
     shares = jnp.exp(ml - jnp.max(ml, axis=0, keepdims=True))
     grand = jnp.sum(shares * pltpu.roll(ml, half, 1), axis=0, keepdims=True)
     in_use = iota(ml.shape, 1) < quarter
     shares = jnp.where(in_use, shares / jnp.where(in_use[0:1], grand, 1.0), 0.0)
     columns = jnp.transpose(shares)
-    arrive(w_copies)
+    w_copies.arrive()
     attended = columns[0:quarter, 0:1] * wbuf[0].astype(F32)
     for j in range(1, KV):
         attended = attended + columns[0:quarter, j : j + 1] * wbuf[j].astype(F32)
@@ -322,20 +355,20 @@
         * hg[...].astype(F32)
     ).astype(BF16)
     nbuf[mine] = normed
-    arrive(spread(lambda peer: nbuf.at[mine], nbuf.at[mine], n_send, n_recv, "kv", (2, 1, KV - 1)))
+    spread(lambda peer: nbuf.at[mine], nbuf.at[mine], n_send, n_recv, "kv", (2, 1, KV - 1)).start().arrive()
     for c in range(4):
         lined_s[c * quarter : (c + 1) * quarter, :] = nbuf[c].astype(F32)
     outs = [lined_s[pl.ds(2 * g, rows, stride=maps), :] for g in range(heads)]
     heads_out = jnp.concatenate(outs, axis=1).astype(BF16)
     ld_wo.wait()
     dbuf[t] = dot(heads_out, wo[...])
-    arrive(spread(lambda peer: dbuf.at[t], dbuf.at[t], d_send, d_recv, "tp"))
+    spread(lambda peer: dbuf.at[t], dbuf.at[t], d_send, d_recv, "tp").start().arrive()
     projected = dbuf[0]
     for j in range(1, TP):
         projected = projected + dbuf[j]
     mixed = (block + projected).astype(BF16).astype(F32)
     sqbuf[z] = to_lanes(jnp.sum(mixed * mixed, axis=1, keepdims=True))
-    s_copies = spread(lambda peer: sqbuf.at[z], sqbuf.at[z], s_send, s_recv, "kv")
+    s_copies = spread(lambda peer: sqbuf.at[z], sqbuf.at[z], s_send, s_recv, "kv").start()
     ld_mg.wait()
     gain2 = jnp.concatenate([mg[k : k + 1, :] for k in range(width // LANES)], axis=1).astype(F32)
     scaled2 = (mixed * gain2).astype(BF16)
@@ -347,13 +380,13 @@
     for j in range(owners):
         us[j] = up[:, j * share_width : (j + 1) * share_width].astype(BF16)
     ur[z] = us[owned]
-    u_copies = spread(lambda peer: us.at[lax.rem(peer, owners)], ur.at[z], u_send, u_recv, "kv")
-    arrive(s_copies)
+    u_copies = spread(lambda peer: us.at[lax.rem(peer, owners)], ur.at[z], u_send, u_recv, "kv").start()
+    s_copies.arrive()
     square2 = sqbuf[0]
     for j in range(1, KV):
         square2 = square2 + sqbuf[j]
     inv2 = to_rows(lax.rsqrt(square2 / D + EPS), rows)
-    arrive(u_copies)
+    u_copies.arrive()
     up_sum = ur[0].astype(F32)
     for j in range(1, KV):
         up_sum = up_sum + ur[j].astype(F32)
@@ -362,18 +395,17 @@
     near = [owners // 2]
     for d in range(owners // 2 - 1, 0, -1):
         near += [d, KV - d]
-    arrive(spread(lambda peer: hbuf.at[owned], hbuf.at[owned], h_send, h_recv, "kv", near))
+    spread(lambda peer: hbuf.at[owned], hbuf.at[owned], h_send, h_recv, "kv", near).start().arrive()
     hidden = jnp.concatenate([hbuf[j] for j in range(owners)], axis=1)
     ld_wd.wait()
     down = dot(hidden, wd[...])
     for k in range(width // LANES):
         fs[k] = down[:, k * LANES : (k + 1) * LANES]
     fr[t] = fs[t // per_tile]
-    earlier = len(started)
-    f_copies = spread(lambda peer: fs.at[peer // per_tile], fr.at[t], f_send, f_recv, "tp")
-    for copy in started[:earlier]:
-        copy.wait_send()
-    arrive(f_copies)
+    f_copies = spread(lambda peer: fs.at[peer // per_tile], fr.at[t], f_send, f_recv, "tp").start()
+    for copies in started[:-1]:
+        copies.sent()
+    f_copies.arrive()
     y = fr[0]
     for j in range(1, TP):
         y = y + fr[j]
@@ -383,8 +415,7 @@
     for k in range(1, per_tile):
         result = jnp.where(lax.rem(t, per_tile) == k, y[:, k * piece : (k + 1) * piece], result)
     out_ref[...] = result.astype(out_ref.dtype)
-    for copy in f_copies:
-        copy.wait_send()
+    f_copies.sent()
 
 
 def body(

time: 83.2 us -> 81.3 us (0.977)
  Pallas kernels: 81.8 us -> 79.9 us
    pallas_call x1, Pallas kernels: 81.8 us -> 79.9 us  [body(): pl.pallas_call(functools.partial(kernel, KV, TP), out_shape=jax.ShapeDtyp...]
where the time goes in v4:
time: 81.3 us; the launch traced here: 81.2 us
  Pallas kernels  79.9 us (98%)
  local copies, waits for them, and re-layouts  1.28 us (2%)
    pallas_call x1, Pallas kernels, body(): pl.pallas_call(functools.partial(kernel, KV, TP), out_shape=jax.ShapeDtyp...  79.9 us

profile of v4, /device:TPU:33, one launch (start us, length us, event | category | flops | bytes accessed | tf_op | source)
XLA Modules:
  0.0 81.2 jit_solution(12234741475167844864)
XLA Ops:
  0.0 79.9 %layer.1 = bf16[16,32]{1,0:T(8,128)(2,1)} custom-call(bf16[16,32]{1,0:T(8,128)(2,1)} %res_h.1, bf16[16,1024,128]{2,1,0:T(8,128)(2,1)} %bitcast.6, bf16[16,1024,128]{2,1,0:T(8,128)(2,1)} %bitcast.7, bf16[2,128]{1,0:T(2,128)(2,1)} %bitcast.8, bf16[256,256]{1,0:T(8,128)(2,1)} %wq_h.1, bf16[256,128]{1,0:T(8,128)(2,1)} %wk_h.1, bf16[256,128]{1,0:T(8,128)(2,1)} %wv_h.1, ...), custom_call_target="tpu_custom_call" | custom-call | tf_op jit(solution)/shard_map/layer/pallas_call | solution.py:465
  79.9 1.3 %copy.15 = bf16[16,32]{1,0:T(8,128)(2,1)} copy(bf16[16,32]{1,0:T(8,128)(2,1)} %layer.1) | data formatting | bytes 2048

commit v5 on v4

--- a/solution.py
+++ b/solution.py
@@ -29,6 +29,20 @@
         return carry
 
     lax.fori_loop(0, n, run, 0)
+
+
+def three(x):
+    high = x.astype(BF16).astype(F32)
+    mid = (x - high).astype(BF16).astype(F32)
+    return high, mid, x - high - mid
+
+
+def stacked(rows):
+    at = iota((8, LANES), 0)
+    out = jnp.zeros((8, LANES), F32)
+    for k, row in enumerate(rows):
+        out = jnp.where(at == k, row, out)
+    return out
 
 
 class Spread:
@@ -102,14 +116,11 @@
     wu,
     wd,
     abuf,
+    qsend,
     qbuf,
-    kvs,
-    kvr,
     lined_s,
     wsend,
     wbuf,
-    mlsend,
-    mlbuf,
     nbuf,
     dbuf,
     sqbuf,
@@ -124,12 +135,8 @@
     a_recv,
     q_send,
     q_recv,
-    r_send,
-    r_recv,
     w_send,
     w_recv,
-    m_send,
-    m_recv,
     n_send,
     n_recv,
     d_send,
@@ -204,14 +211,6 @@
         started.append(out)
         return out
 
-    def start_both(first, second):
-        def step(k):
-            d = first.distances(k)
-            first.copy_to(d).start()
-            second.copy_to(d).start()
-
-        loop(first.steps, step)
-
     ld_res.wait()
     own_piece = res[...].astype(F32)
     tiled = jnp.concatenate([own_piece] * per_tile, axis=1)
@@ -237,16 +236,19 @@
     ld_wk.wait()
     ld_wv.wait()
     proj = dot(scaled, wp[...])
-    qbuf[z] = proj[:, 0:qcols].astype(BF16)
     square = to_lanes(jnp.sum(block * block, axis=1, keepdims=True))
+    extra = stacked((square, square, *three(square)))
+    at = iota((8, LANES), 0)
     for j in range(KV):
-        kvs[j] = jnp.concatenate([proj[j : j + 1, qcols:], square], axis=1)
-    kvr[z] = kvs[z]
+        for g in range(heads):
+            qsend[j, g * rows : (g + 1) * rows, :] = proj[:, g * LANES : (g + 1) * LANES].astype(BF16)
+        key_row = proj[j : j + 1, qcols : qcols + LANES]
+        value_row = proj[j : j + 1, qcols + LANES :]
+        last = jnp.where(at == 0, key_row, jnp.where(at == 1, value_row, extra))
+        qsend[j, heads * rows :, :] = last.astype(BF16)
+    qbuf[z] = qsend[z]
     pl.semaphore_wait(ring_sem.at[1], 2)
-    q_copies = spread(lambda peer: qbuf.at[z], qbuf.at[z], q_send, q_recv, "kv")
-    r_copies = spread(lambda peer: kvs.at[peer], kvr.at[z], r_send, r_recv, "kv")
-
-    start_both(r_copies, q_copies)
+    q_copies = spread(lambda peer: qsend.at[peer], qbuf.at[z], q_send, q_recv, "kv").start()
     ld_keys = load(keys_h, keys, 5)
     ld_values = load(values_h, values, 6)
     ld_lam = load(lam_h, lam, 7)
@@ -256,23 +258,22 @@
     ld_wu = load(wu_h, wu, 11)
     ld_wd = load(wd_h, wd, 12)
     q_copies.arrive()
-    r_copies.arrive()
     q_sum = qbuf[0].astype(F32)
-    r_sum = kvr[0]
     for j in range(1, KV):
         q_sum = q_sum + qbuf[j].astype(F32)
-        r_sum = r_sum + kvr[j]
-    inv_lanes = lax.rsqrt(r_sum[:, 2 * LANES :] / D + EPS)
+    r_sum = q_sum[heads * rows :]
+    inv_lanes = lax.rsqrt((r_sum[2:3] + r_sum[3:4] + r_sum[4:5]) / D + EPS)
     inv_own = jnp.sum(
         jnp.where(iota(inv_lanes.shape, 1) == z, inv_lanes, 0.0), axis=1, keepdims=True
     )
-    new_key = (inv_own * r_sum[:, 0:LANES]).astype(BF16).astype(F32)
-    new_value = (inv_own * r_sum[:, LANES : 2 * LANES]).astype(BF16).astype(F32)
-    query = (to_rows(inv_lanes, rows) * q_sum).astype(BF16)
+    new_key = (inv_own * r_sum[0:1]).astype(BF16).astype(F32)
+    new_value = (inv_own * r_sum[1:2]).astype(BF16).astype(F32)
+    inv_rows = to_rows(inv_lanes, rows)
 
     lane = iota((rows, LANES), 1)
     for g in range(heads):
-        head = query[:, g * LANES : (g + 1) * LANES].astype(F32) * (1.0 / half**0.5)
+        head = (inv_rows * q_sum[g * rows : (g + 1) * rows]).astype(BF16)
+        head = head.astype(F32) * (1.0 / half**0.5)
         for c in range(2):
             lined_s[pl.ds(2 * g + c, rows, stride=maps), :] = jnp.where(lane // half == c, head, 0.0)
     lined = lined_s[...]
@@ -318,29 +319,25 @@
     weighted = weighted * old_part + own_part * new_value
     quarter = lines // 4
     mine = lax.rem(z, 4)
-    lane = iota((quarter, LANES), 1)
-    line = iota((quarter, LANES), 0)
     for c in range(4):
         at = slice(c * quarter, (c + 1) * quarter)
-        wsend[c] = weighted[at].astype(BF16)
-        both = jnp.where(lane == line, new_top[at], jnp.where(lane == line + half, total[at], 0.0))
-        mlsend[c] = jnp.sum(both, axis=0, keepdims=True)
+        wsend[c, 0:quarter, :] = weighted[at].astype(BF16)
+        both = stacked((*three(to_lanes(new_top[at])), *three(to_lanes(total[at]))))
+        wsend[c, quarter:, :] = both.astype(BF16)
     wbuf[z] = wsend[mine]
-    mlbuf[z] = mlsend[mine]
-    m_copies = spread(lambda peer: mlsend.at[lax.rem(peer, 4)], mlbuf.at[z], m_send, m_recv, "kv")
-    w_copies = spread(lambda peer: wsend.at[lax.rem(peer, 4)], wbuf.at[z], w_send, w_recv, "kv")
-    start_both(m_copies, w_copies)
-    m_copies.arrive()
-    ml = jnp.concatenate([mlbuf[j] for j in range(KV)], axis=0)
+    w_copies = spread(lambda peer: wsend.at[lax.rem(peer, 4)], wbuf.at[z], w_send, w_recv, "kv").start()
+    w_copies.arrive()
+    tails = [wbuf[j, quarter:, :].astype(F32) for j in range(KV)]
+    ml = jnp.concatenate([x[0:1] + x[1:2] + x[2:3] for x in tails], axis=0)
+    totals = jnp.concatenate([x[3:4] + x[4:5] + x[5:6] for x in tails], axis=0)
     shares = jnp.exp(ml - jnp.max(ml, axis=0, keepdims=True))
-    grand = jnp.sum(shares * pltpu.roll(ml, half, 1), axis=0, keepdims=True)
+    grand = jnp.sum(shares * totals, axis=0, keepdims=True)
     in_use = iota(ml.shape, 1) < quarter
     shares = jnp.where(in_use, shares / jnp.where(in_use[0:1], grand, 1.0), 0.0)
     columns = jnp.transpose(shares)
-    w_copies.arrive()
-    attended = columns[0:quarter, 0:1] * wbuf[0].astype(F32)
+    attended = columns[0:quarter, 0:1] * wbuf[0, 0:quarter, :].astype(F32)
     for j in range(1, KV):
-        attended = attended + columns[0:quarter, j : j + 1] * wbuf[j].astype(F32)
+        attended = attended + columns[0:quarter, j : j + 1] * wbuf[j, 0:quarter, :].astype(F32)
     ld_lam.wait()
     ld_hg.wait()
     lambdas = lam[0:1, 0:1]
@@ -368,7 +365,6 @@
         projected = projected + dbuf[j]
     mixed = (block + projected).astype(BF16).astype(F32)
     sqbuf[z] = to_lanes(jnp.sum(mixed * mixed, axis=1, keepdims=True))
-    s_copies = spread(lambda peer: sqbuf.at[z], sqbuf.at[z], s_send, s_recv, "kv").start()
     ld_mg.wait()
     gain2 = jnp.concatenate([mg[k : k + 1, :] for k in range(width // LANES)], axis=1).astype(F32)
     scaled2 = (mixed * gain2).astype(BF16)
@@ -381,16 +377,12 @@
         us[j] = up[:, j * share_width : (j + 1) * share_width].astype(BF16)
     ur[z] = us[owned]
     u_copies = spread(lambda peer: us.at[lax.rem(peer, owners)], ur.at[z], u_send, u_recv, "kv").start()
-    s_copies.arrive()
-    square2 = sqbuf[0]
-    for j in range(1, KV):
-        square2 = square2 + sqbuf[j]
-    inv2 = to_rows(lax.rsqrt(square2 / D + EPS), rows)
+    s_copies = spread(lambda peer: sqbuf.at[z], sqbuf.at[z], s_send, s_recv, "kv").start()
     u_copies.arrive()
     up_sum = ur[0].astype(F32)
     for j in range(1, KV):
         up_sum = up_sum + ur[j].astype(F32)
-    act = jnp.maximum(inv2 * up_sum, 0.0)
+    act = jnp.maximum(up_sum, 0.0)
     hbuf[owned] = (act * act).astype(BF16)
     near = [owners // 2]
     for d in range(owners // 2 - 1, 0, -1):
@@ -405,10 +397,16 @@
     f_copies = spread(lambda peer: fs.at[peer // per_tile], fr.at[t], f_send, f_recv, "tp").start()
     for copies in started[:-1]:
         copies.sent()
+    s_copies.arrive()
+    square2 = sqbuf[0]
+    for j in range(1, KV):
+        square2 = square2 + sqbuf[j]
+    inv2 = to_rows(1.0 / (square2 / D + EPS), rows)
     f_copies.arrive()
     y = fr[0]
     for j in range(1, TP):
         y = y + fr[j]
+    y = inv2 * y
     for k in range(width // LANES):
         y = y + jnp.where(t // per_tile == k, mixed[:, k * LANES : (k + 1) * LANES], 0.0)
     result = y[:, 0:piece]
@@ -480,14 +478,11 @@
             pltpu.VMEM(up_weight.shape, BF16),
             pltpu.VMEM(down_weight.shape, BF16),
             pltpu.VMEM((TP, rows, LANES), BF16),
-            pltpu.VMEM((KV, rows, qcols), BF16),
-            pltpu.VMEM((KV, 1, 3 * LANES), F32),
-            pltpu.VMEM((KV, 1, 3 * LANES), F32),
+            pltpu.VMEM((KV, rows * qcols // LANES + 8, LANES), BF16),
+            pltpu.VMEM((KV, rows * qcols // LANES + 8, LANES), BF16),
             pltpu.VMEM((lines, LANES), F32),
-            pltpu.VMEM((4, lines // 4, LANES), BF16),
-            pltpu.VMEM((KV, lines // 4, LANES), BF16),
-            pltpu.VMEM((4, 1, LANES), F32),
-            pltpu.VMEM((KV, 1, LANES), F32),
+            pltpu.VMEM((4, lines // 4 + 8, LANES), BF16),
+            pltpu.VMEM((KV, lines // 4 + 8, LANES), BF16),
             pltpu.VMEM((4, lines // 4, LANES), BF16),
             pltpu.VMEM((TP, rows, width), F32),
             pltpu.VMEM((KV, 1, LANES), F32),
@@ -499,8 +494,6 @@
             pltpu.SemaphoreType.REGULAR((2,)),
             dma((13,)),
             *tp_sems,
-            *kv_sems,
-            *kv_sems,
             *kv_sems,
             *kv_sems,
             *kv_sems,

time: 81.3 us -> 80.1 us (0.985)
  Pallas kernels: 79.9 us -> 78.7 us
    pallas_call x1, Pallas kernels: 79.9 us -> 78.7 us  [body(): pl.pallas_call(functools.partial(kernel, KV, TP), out_shape=jax.ShapeDtyp...]
where the time goes in v5:
time: 80.1 us; the launch traced here: 80 us
  Pallas kernels  78.7 us (98%)
  local copies, waits for them, and re-layouts  1.28 us (2%)
    pallas_call x1, Pallas kernels, body(): pl.pallas_call(functools.partial(kernel, KV, TP), out_shape=jax.ShapeDtyp...  78.7 us

profile of v5, /device:TPU:33, one launch (start us, length us, event | category | flops | bytes accessed | tf_op | source)
XLA Modules:
  0.0 80.0 jit_solution(16724135101018486191)
XLA Ops:
  0.0 78.7 %layer.1 = bf16[16,32]{1,0:T(8,128)(2,1)} custom-call(bf16[16,32]{1,0:T(8,128)(2,1)} %res_h.1, bf16[16,1024,128]{2,1,0:T(8,128)(2,1)} %bitcast.6, bf16[16,1024,128]{2,1,0:T(8,128)(2,1)} %bitcast.7, bf16[2,128]{1,0:T(2,128)(2,1)} %bitcast.8, bf16[256,256]{1,0:T(8,128)(2,1)} %wq_h.1, bf16[256,128]{1,0:T(8,128)(2,1)} %wk_h.1, bf16[256,128]{1,0:T(8,128)(2,1)} %wv_h.1, ...), custom_call_target="tpu_custom_call" | custom-call | tf_op jit(solution)/shard_map/layer/pallas_call | solution.py:463
  78.7 1.3 %copy.15 = bf16[16,32]{1,0:T(8,128)(2,1)} copy(bf16[16,32]{1,0:T(8,128)(2,1)} %layer.1) | data formatting | bytes 2048

commit v6 on v5

--- a/solution.py
+++ b/solution.py
@@ -46,25 +46,21 @@
 
 
 class Spread:
-    def __init__(self, copy_to, distances, steps):
+    def __init__(self, copy, copy_to, distances, steps, peer, slots):
         self.copy_to, self.distances, self.steps = copy_to, distances, steps
-
-    def each(self, act):
+        self.whole = copy(slots, slots, peer)
+
+    def start(self):
         if self.steps is None:
             for d in self.distances:
-                act(self.copy_to(d))
+                self.copy_to(d).start()
         else:
-            loop(self.steps, lambda k: act(self.copy_to(self.distances(k))))
-
-    def start(self):
-        self.each(lambda copy: copy.start())
+            loop(self.steps, lambda k: self.copy_to(self.distances(k)).start())
         return self
 
     def arrive(self):
-        self.each(lambda copy: copy.wait_recv())
-
-    def sent(self):
-        self.each(lambda copy: copy.wait_send())
+        self.whole.wait_recv()
+        self.whole.wait_send()
 
 
 def iota(shape, dim):
@@ -131,24 +127,8 @@
     fr,
     ring_sem,
     load_sem,
-    a_send,
-    a_recv,
-    q_send,
-    q_recv,
-    w_send,
-    w_recv,
-    n_send,
-    n_recv,
-    d_send,
-    d_recv,
-    s_send,
-    s_recv,
-    u_send,
-    u_recv,
-    h_send,
-    h_recv,
-    f_send,
-    f_recv,
+    send_sem,
+    recv_sem,
 ):
     z = lax.axis_index("kv")
     t = lax.axis_index("tp")
@@ -188,28 +168,28 @@
     ld_wk = load(wk_h, wp.at[:, qcols : qcols + LANES], 3)
     ld_wv = load(wv_h, wp.at[:, qcols + LANES : qcols + 2 * LANES], 4)
 
-    started = []
-
-    def spread(src_of, dst, ssem, rsem, axis, distances=None):
+    def spread(src_of, dst, buf, ssem, rsem, axis, distances=None):
         me, n = (z, KV) if axis == "kv" else (t, TP)
-
-        def copy_to(d):
-            peer = lax.rem(me + d, n)
+        steps = n - 1 if distances is None else None
+        count = n - 1 if distances is None else len(distances)
+
+        def copy(src, dst, peer):
             return pltpu.make_async_remote_copy(
-                src_ref=src_of(peer),
+                src_ref=src,
                 dst_ref=dst,
-                send_sem=ssem.at[d - 1],
-                recv_sem=rsem.at[d - 1],
+                send_sem=ssem,
+                recv_sem=rsem,
                 device_id={axis: peer},
                 device_id_type=MESH,
             )
 
-        if distances is None:
-            out = Spread(copy_to, far_first(n), n - 1)
-        else:
-            out = Spread(copy_to, distances, None)
-        started.append(out)
-        return out
+        def copy_to(d):
+            peer = lax.rem(me + d, n)
+            return copy(src_of(peer), dst, peer)
+
+        order = far_first(n) if distances is None else distances
+        slots = buf.at[pl.ds(0, count)]
+        return Spread(copy, copy_to, order, steps, lax.rem(me + 1, n), slots)
 
     ld_res.wait()
     own_piece = res[...].astype(F32)
@@ -217,7 +197,7 @@
     at = iota(tiled.shape, 1) // piece == lax.rem(t, per_tile)
     abuf[t] = jnp.where(at, tiled, 0.0).astype(BF16)
     pl.semaphore_wait(barrier, TP - 1 + 4)
-    a_copies = spread(lambda peer: abuf.at[t], abuf.at[t], a_send, a_recv, "tp").start()
+    a_copies = spread(lambda peer: abuf.at[t], abuf.at[t], abuf, send_sem.at[0], recv_sem.at[0], "tp").start()
     both_ways(ring_sem.at[0], 2)
     pl.semaphore_wait(ring_sem.at[0], 2)
     both_ways(ring_sem.at[1], 4)
@@ -248,15 +228,15 @@
         qsend[j, heads * rows :, :] = last.astype(BF16)
     qbuf[z] = qsend[z]
     pl.semaphore_wait(ring_sem.at[1], 2)
-    q_copies = spread(lambda peer: qsend.at[peer], qbuf.at[z], q_send, q_recv, "kv").start()
-    ld_keys = load(keys_h, keys, 5)
-    ld_values = load(values_h, values, 6)
-    ld_lam = load(lam_h, lam, 7)
-    ld_hg = load(hg_h, hg, 8)
-    ld_wo = load(wo_h, wo, 9)
-    ld_mg = load(mg_h, mg, 10)
-    ld_wu = load(wu_h, wu, 11)
-    ld_wd = load(wd_h, wd, 12)
+    q_copies = spread(lambda peer: qsend.at[peer], qbuf.at[z], qbuf, send_sem.at[0], recv_sem.at[1], "kv").start()
+    ld_keys = load(keys_h, keys, 0)
+    ld_values = load(values_h, values, 1)
+    ld_lam = load(lam_h, lam, 2)
+    ld_hg = load(hg_h, hg, 3)
+    ld_wo = load(wo_h, wo, 4)
+    ld_mg = load(mg_h, mg, 5)
+    ld_wu = load(wu_h, wu, 6)
+    ld_wd = load(wd_h, wd, 7)
     q_copies.arrive()
     q_sum = qbuf[0].astype(F32)
     for j in range(1, KV):
@@ -325,7 +305,7 @@
         both = stacked((*three(to_lanes(new_top[at])), *three(to_lanes(total[at]))))
         wsend[c, quarter:, :] = both.astype(BF16)
     wbuf[z] = wsend[mine]
-    w_copies = spread(lambda peer: wsend.at[lax.rem(peer, 4)], wbuf.at[z], w_send, w_recv, "kv").start()
+    w_copies = spread(lambda peer: wsend.at[lax.rem(peer, 4)], wbuf.at[z], wbuf, send_sem.at[0], recv_sem.at[2], "kv").start()
     w_copies.arrive()
     tails = [wbuf[j, quarter:, :].astype(F32) for j in range(KV)]
     ml = jnp.concatenate([x[0:1] + x[1:2] + x[2:3] for x in tails], axis=0)
@@ -352,14 +332,14 @@
         * hg[...].astype(F32)
     ).astype(BF16)
     nbuf[mine] = normed
-    spread(lambda peer: nbuf.at[mine], nbuf.at[mine], n_send, n_recv, "kv", (2, 1, KV - 1)).start().arrive()
+    spread(lambda peer: nbuf.at[mine], nbuf.at[mine], nbuf, send_sem.at[0], recv_sem.at[3], "kv", (2, 1, KV - 1)).start().arrive()
     for c in range(4):
         lined_s[c * quarter : (c + 1) * quarter, :] = nbuf[c].astype(F32)
     outs = [lined_s[pl.ds(2 * g, rows, stride=maps), :] for g in range(heads)]
     heads_out = jnp.concatenate(outs, axis=1).astype(BF16)
     ld_wo.wait()
     dbuf[t] = dot(heads_out, wo[...])
-    spread(lambda peer: dbuf.at[t], dbuf.at[t], d_send, d_recv, "tp").start().arrive()
+    spread(lambda peer: dbuf.at[t], dbuf.at[t], dbuf, send_sem.at[0], recv_sem.at[4], "tp").start().arrive()
     projected = dbuf[0]
     for j in range(1, TP):
         projected = projected + dbuf[j]
@@ -376,8 +356,8 @@
     for j in range(owners):
         us[j] = up[:, j * share_width : (j + 1) * share_width].astype(BF16)
     ur[z] = us[owned]
-    u_copies = spread(lambda peer: us.at[lax.rem(peer, owners)], ur.at[z], u_send, u_recv, "kv").start()
-    s_copies = spread(lambda peer: sqbuf.at[z], sqbuf.at[z], s_send, s_recv, "kv").start()
+    u_copies = spread(lambda peer: us.at[lax.rem(peer, owners)], ur.at[z], ur, send_sem.at[0], recv_sem.at[5], "kv").start()
+    s_copies = spread(lambda peer: sqbuf.at[z], sqbuf.at[z], sqbuf, send_sem.at[1], recv_sem.at[6], "kv").start()
     u_copies.arrive()
     up_sum = ur[0].astype(F32)
     for j in range(1, KV):
@@ -387,16 +367,14 @@
     near = [owners // 2]
     for d in range(owners // 2 - 1, 0, -1):
         near += [d, KV - d]
-    spread(lambda peer: hbuf.at[owned], hbuf.at[owned], h_send, h_recv, "kv", near).start().arrive()
+    spread(lambda peer: hbuf.at[owned], hbuf.at[owned], hbuf, send_sem.at[0], recv_sem.at[7], "kv", near).start().arrive()
     hidden = jnp.concatenate([hbuf[j] for j in range(owners)], axis=1)
     ld_wd.wait()
     down = dot(hidden, wd[...])
     for k in range(width // LANES):
         fs[k] = down[:, k * LANES : (k + 1) * LANES]
     fr[t] = fs[t // per_tile]
-    f_copies = spread(lambda peer: fs.at[peer // per_tile], fr.at[t], f_send, f_recv, "tp").start()
-    for copies in started[:-1]:
-        copies.sent()
+    f_copies = spread(lambda peer: fs.at[peer // per_tile], fr.at[t], fr, send_sem.at[0], recv_sem.at[8], "tp").start()
     s_copies.arrive()
     square2 = sqbuf[0]
     for j in range(1, KV):
@@ -413,7 +391,6 @@
     for k in range(1, per_tile):
         result = jnp.where(lax.rem(t, per_tile) == k, y[:, k * piece : (k + 1) * piece], result)
     out_ref[...] = result.astype(out_ref.dtype)
-    f_copies.sent()
 
 
 def body(
@@ -458,8 +435,6 @@
         up_weight,
         down_weight,
     )
-    kv_sems = [dma((KV - 1,))] * 2
-    tp_sems = [dma((TP - 1,))] * 2
     return pl.pallas_call(
         functools.partial(kernel, KV, TP),
         out_shape=jax.ShapeDtypeStruct((rows, piece), residual.dtype),
@@ -492,16 +467,9 @@
             pltpu.VMEM((width // LANES, rows, LANES), F32),
             pltpu.VMEM((TP, rows, LANES), F32),
             pltpu.SemaphoreType.REGULAR((2,)),
-            dma((13,)),
-            *tp_sems,
-            *kv_sems,
-            *kv_sems,
-            *kv_sems,
-            *tp_sems,
-            *kv_sems,
-            *kv_sems,
-            *kv_sems,
-            *tp_sems,
+            dma((8,)),
+            dma((2,)),
+            dma((9,)),
         ],
         compiler_params=pltpu.CompilerParams(
             collective_id=0, has_side_effects=True, vmem_limit_bytes=64 * 1000 * 1000

time: 80.1 us -> 78.3 us (0.978)
  Pallas kernels: 78.7 us -> 76.9 us
    pallas_call x1, Pallas kernels: 78.7 us -> 76.9 us  [body(): pl.pallas_call(functools.partial(kernel, KV, TP), out_shape=jax.ShapeDtyp...]
where the time goes in v6:
time: 78.3 us; the launch traced here: 78.2 us
  Pallas kernels  76.9 us (98%)
  local copies, waits for them, and re-layouts  1.28 us (2%)
    pallas_call x1, Pallas kernels, body(): pl.pallas_call(functools.partial(kernel, KV, TP), out_shape=jax.ShapeDtyp...  76.9 us

profile of v6, /device:TPU:33, one launch (start us, length us, event | category | flops | bytes accessed | tf_op | source)
XLA Modules:
  0.0 78.2 jit_solution(15478588273368005492)
XLA Ops:
  0.0 76.9 %layer.1 = bf16[16,32]{1,0:T(8,128)(2,1)} custom-call(bf16[16,32]{1,0:T(8,128)(2,1)} %res_h.1, bf16[16,1024,128]{2,1,0:T(8,128)(2,1)} %bitcast.6, bf16[16,1024,128]{2,1,0:T(8,128)(2,1)} %bitcast.7, bf16[2,128]{1,0:T(2,128)(2,1)} %bitcast.8, bf16[256,256]{1,0:T(8,128)(2,1)} %wq_h.1, bf16[256,128]{1,0:T(8,128)(2,1)} %wk_h.1, bf16[256,128]{1,0:T(8,128)(2,1)} %wv_h.1, ...), custom_call_target="tpu_custom_call" | custom-call | tf_op jit(solution)/shard_map/layer/pallas_call | solution.py:438
  76.9 1.3 %copy.15 = bf16[16,32]{1,0:T(8,128)(2,1)} copy(bf16[16,32]{1,0:T(8,128)(2,1)} %layer.1) | data formatting | bytes 2048

commit v7 on v6

--- a/solution.py
+++ b/solution.py
@@ -261,31 +261,24 @@
     ld_keys.wait()
     ld_values.wait()
     tops, totals, sums = [], [], []
+    seqs = 8 // maps
+    group = iota((8, LANES), 0) // maps
     for p in range(lines // 8):
-        seqs = 8 // maps
-        qp = lined[8 * p : 8 * p + 8, :].astype(BF16)
-        scores = None
-        for k in range(seqs):
-            part = lax.dot_general(
-                qp, keys[seqs * p + k], (((1,), (1,)), ((), ())), preferred_element_type=F32
-            )
-            if scores is None:
-                scores = part
-            else:
-                scores = jnp.where(iota(part.shape, 0) // maps == k, part, scores)
+        qp = lined[8 * p : 8 * p + 8, :]
+        wide = jnp.concatenate([jnp.where(group == k, qp, 0.0) for k in range(seqs)], axis=1)
+        wide_keys = jnp.concatenate([keys[seqs * p + k] for k in range(seqs)], axis=1)
+        scores = lax.dot_general(
+            wide.astype(BF16), wide_keys, (((1,), (1,)), ((), ())), preferred_element_type=F32
+        )
         top = jnp.max(scores, axis=1, keepdims=True)
         expo = jnp.exp(scores - top)
-        total = jnp.sum(expo, axis=1, keepdims=True)
-        probs = expo.astype(BF16)
-        weighted = None
-        for k in range(seqs):
-            part = dot(probs, values[seqs * p + k])
-            if weighted is None:
-                weighted = part
-            else:
-                weighted = jnp.where(iota(part.shape, 0) // maps == k, part, weighted)
+        wide_values = jnp.concatenate([values[seqs * p + k] for k in range(seqs)], axis=1)
+        part = dot(expo.astype(BF16), wide_values)
+        weighted = part[:, 0:LANES]
+        for k in range(1, seqs):
+            weighted = jnp.where(group == k, part[:, k * LANES : (k + 1) * LANES], weighted)
         tops.append(top)
-        totals.append(total)
+        totals.append(jnp.sum(expo, axis=1, keepdims=True))
         sums.append(weighted)
     top = jnp.concatenate(tops, axis=0)
     total = jnp.concatenate(totals, axis=0)
@@ -338,11 +331,11 @@
     outs = [lined_s[pl.ds(2 * g, rows, stride=maps), :] for g in range(heads)]
     heads_out = jnp.concatenate(outs, axis=1).astype(BF16)
     ld_wo.wait()
-    dbuf[t] = dot(heads_out, wo[...])
+    dbuf[t] = dot(heads_out, wo[...]).astype(BF16)
     spread(lambda peer: dbuf.at[t], dbuf.at[t], dbuf, send_sem.at[0], recv_sem.at[4], "tp").start().arrive()
-    projected = dbuf[0]
+    projected = dbuf[0].astype(F32)
     for j in range(1, TP):
-        projected = projected + dbuf[j]
+        projected = projected + dbuf[j].astype(F32)
     mixed = (block + projected).astype(BF16).astype(F32)
     sqbuf[z] = to_lanes(jnp.sum(mixed * mixed, axis=1, keepdims=True))
     ld_mg.wait()
@@ -357,7 +350,6 @@
         us[j] = up[:, j * share_width : (j + 1) * share_width].astype(BF16)
     ur[z] = us[owned]
     u_copies = spread(lambda peer: us.at[lax.rem(peer, owners)], ur.at[z], ur, send_sem.at[0], recv_sem.at[5], "kv").start()
-    s_copies = spread(lambda peer: sqbuf.at[z], sqbuf.at[z], sqbuf, send_sem.at[1], recv_sem.at[6], "kv").start()
     u_copies.arrive()
     up_sum = ur[0].astype(F32)
     for j in range(1, KV):
@@ -367,7 +359,9 @@
     near = [owners // 2]
     for d in range(owners // 2 - 1, 0, -1):
         near += [d, KV - d]
-    spread(lambda peer: hbuf.at[owned], hbuf.at[owned], hbuf, send_sem.at[0], recv_sem.at[7], "kv", near).start().arrive()
+    h_copies = spread(lambda peer: hbuf.at[owned], hbuf.at[owned], hbuf, send_sem.at[0], recv_sem.at[7], "kv", near).start()
+    s_copies = spread(lambda peer: sqbuf.at[z], sqbuf.at[z], sqbuf, send_sem.at[1], recv_sem.at[6], "kv").start()
+    h_copies.arrive()
     hidden = jnp.concatenate([hbuf[j] for j in range(owners)], axis=1)
     ld_wd.wait()
     down = dot(hidden, wd[...])
@@ -459,7 +453,7 @@
             pltpu.VMEM((4, lines // 4 + 8, LANES), BF16),
             pltpu.VMEM((KV, lines // 4 + 8, LANES), BF16),
             pltpu.VMEM((4, lines // 4, LANES), BF16),
-            pltpu.VMEM((TP, rows, width), F32),
+            pltpu.VMEM((TP, rows, width), BF16),
             pltpu.VMEM((KV, 1, LANES), F32),
             pltpu.VMEM((KV // 2, rows, share), BF16),
             pltpu.VMEM((KV, rows, share), BF16),

time: 78.3 us -> 78 us (level)
  no operation moved by 1% of the time
where the time goes in v7:
time: 78 us; the launch traced here: 77.8 us
  Pallas kernels  76.5 us (98%)
  local copies, waits for them, and re-layouts  1.28 us (2%)
    pallas_call x1, Pallas kernels, body(): pl.pallas_call(functools.partial(kernel, KV, TP), out_shape=jax.ShapeDtyp...  76.5 us

profile of v7, /device:TPU:33, one launch (start us, length us, event | category | flops | bytes accessed | tf_op | source)
XLA Modules:
  0.0 77.8 jit_solution(13969746541947283586)
XLA Ops:
  0.0 76.5 %layer.1 = bf16[16,32]{1,0:T(8,128)(2,1)} custom-call(bf16[16,32]{1,0:T(8,128)(2,1)} %res_h.1, bf16[16,1024,128]{2,1,0:T(8,128)(2,1)} %bitcast.6, bf16[16,1024,128]{2,1,0:T(8,128)(2,1)} %bitcast.7, bf16[2,128]{1,0:T(2,128)(2,1)} %bitcast.8, bf16[256,256]{1,0:T(8,128)(2,1)} %wq_h.1, bf16[256,128]{1,0:T(8,128)(2,1)} %wk_h.1, bf16[256,128]{1,0:T(8,128)(2,1)} %wv_h.1, ...), custom_call_target="tpu_custom_call" | custom-call | tf_op jit(solution)/shard_map/layer/pallas_call | solution.py:432
  76.5 1.3 %copy.15 = bf16[16,32]{1,0:T(8,128)(2,1)} copy(bf16[16,32]{1,0:T(8,128)(2,1)} %layer.1) | data formatting | bytes 2048

commit v8 on v7

--- a/solution.py
+++ b/solution.py
@@ -48,19 +48,21 @@
 class Spread:
     def __init__(self, copy, copy_to, distances, steps, peer, slots):
         self.copy_to, self.distances, self.steps = copy_to, distances, steps
-        self.whole = copy(slots, slots, peer)
-
-    def start(self):
+        self.whole = lambda: copy(slots, slots, peer)
+
+    def start(self, first=0, last=None):
         if self.steps is None:
             for d in self.distances:
                 self.copy_to(d).start()
         else:
-            loop(self.steps, lambda k: self.copy_to(self.distances(k)).start())
+            steps = (self.steps if last is None else last) - first
+            loop(steps, lambda k: self.copy_to(self.distances(k + first)).start())
         return self
 
     def arrive(self):
-        self.whole.wait_recv()
-        self.whole.wait_send()
+        whole = self.whole()
+        whole.wait_recv()
+        whole.wait_send()
 
 
 def iota(shape, dim):
@@ -227,8 +229,11 @@
         last = jnp.where(at == 0, key_row, jnp.where(at == 1, value_row, extra))
         qsend[j, heads * rows :, :] = last.astype(BF16)
     qbuf[z] = qsend[z]
+    q_copies = spread(lambda peer: qsend.at[peer], qbuf.at[z], qbuf, send_sem.at[0], recv_sem.at[1], "kv")
+    far = KV // 2 - 1
+    q_copies.start(far)
     pl.semaphore_wait(ring_sem.at[1], 2)
-    q_copies = spread(lambda peer: qsend.at[peer], qbuf.at[z], qbuf, send_sem.at[0], recv_sem.at[1], "kv").start()
+    q_copies.start(0, far)
     ld_keys = load(keys_h, keys, 0)
     ld_values = load(values_h, values, 1)
     ld_lam = load(lam_h, lam, 2)
@@ -256,49 +261,55 @@
         head = head.astype(F32) * (1.0 / half**0.5)
         for c in range(2):
             lined_s[pl.ds(2 * g + c, rows, stride=maps), :] = jnp.where(lane // half == c, head, 0.0)
-    lined = lined_s[...]
 
     ld_keys.wait()
     ld_values.wait()
-    tops, totals, sums = [], [], []
     seqs = 8 // maps
     group = iota((8, LANES), 0) // maps
-    for p in range(lines // 8):
-        qp = lined[8 * p : 8 * p + 8, :]
-        wide = jnp.concatenate([jnp.where(group == k, qp, 0.0) for k in range(seqs)], axis=1)
-        wide_keys = jnp.concatenate([keys[seqs * p + k] for k in range(seqs)], axis=1)
-        scores = lax.dot_general(
-            wide.astype(BF16), wide_keys, (((1,), (1,)), ((), ())), preferred_element_type=F32
-        )
-        top = jnp.max(scores, axis=1, keepdims=True)
-        expo = jnp.exp(scores - top)
-        wide_values = jnp.concatenate([values[seqs * p + k] for k in range(seqs)], axis=1)
-        part = dot(expo.astype(BF16), wide_values)
-        weighted = part[:, 0:LANES]
-        for k in range(1, seqs):
-            weighted = jnp.where(group == k, part[:, k * LANES : (k + 1) * LANES], weighted)
-        tops.append(top)
-        totals.append(jnp.sum(expo, axis=1, keepdims=True))
-        sums.append(weighted)
-    top = jnp.concatenate(tops, axis=0)
-    total = jnp.concatenate(totals, axis=0)
-    weighted = jnp.concatenate(sums, axis=0)
-    own = jnp.sum(lined * new_key, axis=1, keepdims=True)
-    own = jnp.where(iota(own.shape, 0) // maps == z, own, LOW)
-    new_top = jnp.maximum(top, own)
-    old_part = jnp.exp(top - new_top)
-    own_part = jnp.exp(own - new_top)
-    total = total * old_part + own_part
-    weighted = weighted * old_part + own_part * new_value
     quarter = lines // 4
     mine = lax.rem(z, 4)
-    for c in range(4):
-        at = slice(c * quarter, (c + 1) * quarter)
-        wsend[c, 0:quarter, :] = weighted[at].astype(BF16)
-        both = stacked((*three(to_lanes(new_top[at])), *three(to_lanes(total[at]))))
-        wsend[c, quarter:, :] = both.astype(BF16)
-    wbuf[z] = wsend[mine]
-    w_copies = spread(lambda peer: wsend.at[lax.rem(peer, 4)], wbuf.at[z], wbuf, send_sem.at[0], recv_sem.at[2], "kv").start()
+    for r in (0, 3, 1, 2):
+        part_of = lax.rem(mine + r, 4)
+        tops, totals, sums = [], [], []
+        for u in range(quarter // 8):
+            p = part_of * (quarter // 8) + u
+            qp = lined_s[pl.ds(pl.multiple_of(8 * p, 8), 8), :]
+            wide = jnp.concatenate([jnp.where(group == k, qp, 0.0) for k in range(seqs)], axis=1)
+            wide_keys = jnp.concatenate([keys[seqs * p + k] for k in range(seqs)], axis=1)
+            scores = lax.dot_general(
+                wide.astype(BF16), wide_keys, (((1,), (1,)), ((), ())), preferred_element_type=F32
+            )
+            top = jnp.max(scores, axis=1, keepdims=True)
+            expo = jnp.exp(scores - top)
+            wide_values = jnp.concatenate([values[seqs * p + k] for k in range(seqs)], axis=1)
+            part = dot(expo.astype(BF16), wide_values)
+            weighted = part[:, 0:LANES]
+            for k in range(1, seqs):
+                weighted = jnp.where(group == k, part[:, k * LANES : (k + 1) * LANES], weighted)
+            tops.append(top)
+            totals.append(jnp.sum(expo, axis=1, keepdims=True))
+            sums.append(weighted)
+        top = jnp.concatenate(tops, axis=0)
+        total = jnp.concatenate(totals, axis=0)
+        weighted = jnp.concatenate(sums, axis=0)
+        queries = lined_s[pl.ds(pl.multiple_of(quarter * part_of, quarter), quarter), :]
+        own = jnp.sum(queries * new_key, axis=1, keepdims=True)
+        sequence = part_of * (quarter // maps) + iota(own.shape, 0) // maps
+        own = jnp.where(sequence == z, own, LOW)
+        new_top = jnp.maximum(top, own)
+        old_part = jnp.exp(top - new_top)
+        own_part = jnp.exp(own - new_top)
+        total = total * old_part + own_part
+        weighted = weighted * old_part + own_part * new_value
+        wsend[r, 0:quarter, :] = weighted.astype(BF16)
+        both = stacked((*three(to_lanes(new_top)), *three(to_lanes(total))))
+        wsend[r, quarter:, :] = both.astype(BF16)
+        reach = sorted(range(r if r else 4, KV, 4), key=lambda d: -min(d, KV - d))
+        spread(
+            lambda peer: wsend.at[r], wbuf.at[z], wbuf, send_sem.at[0], recv_sem.at[2], "kv", reach
+        ).start()
+    wbuf[z] = wsend[0]
+    w_copies = spread(lambda peer: wsend.at[0], wbuf.at[z], wbuf, send_sem.at[0], recv_sem.at[2], "kv")
     w_copies.arrive()
     tails = [wbuf[j, quarter:, :].astype(F32) for j in range(KV)]
     ml = jnp.concatenate([x[0:1] + x[1:2] + x[2:3] for x in tails], axis=0)

time: 78 us -> 78.5 us (level)
  no operation moved by 1% of the time
where the time goes in v8:
time: 78.5 us; the launch traced here: 78.4 us
  Pallas kernels  77.1 us (98%)
  local copies, waits for them, and re-layouts  1.28 us (2%)
    pallas_call x1, Pallas kernels, body(): pl.pallas_call(functools.partial(kernel, KV, TP), out_shape=jax.ShapeDtyp...  77.1 us

profile of v8, /device:TPU:33, one launch (start us, length us, event | category | flops | bytes accessed | tf_op | source)
XLA Modules:
  0.0 78.4 jit_solution(1792158033068561394)
XLA Ops:
  0.0 77.1 %layer.1 = bf16[16,32]{1,0:T(8,128)(2,1)} custom-call(bf16[16,32]{1,0:T(8,128)(2,1)} %res_h.1, bf16[16,1024,128]{2,1,0:T(8,128)(2,1)} %bitcast.6, bf16[16,1024,128]{2,1,0:T(8,128)(2,1)} %bitcast.7, bf16[2,128]{1,0:T(2,128)(2,1)} %bitcast.8, bf16[256,256]{1,0:T(8,128)(2,1)} %wq_h.1, bf16[256,128]{1,0:T(8,128)(2,1)} %wk_h.1, bf16[256,128]{1,0:T(8,128)(2,1)} %wv_h.1, ...), custom_call_target="tpu_custom_call" | custom-call | tf_op jit(solution)/shard_map/layer/pallas_call | solution.py:443
  77.1 1.3 %copy.15 = bf16[16,32]{1,0:T(8,128)(2,1)} copy(bf16[16,32]{1,0:T(8,128)(2,1)} %layer.1) | data formatting | bytes 2048

commit v9 on v8

--- a/solution.py
+++ b/solution.py
@@ -50,13 +50,12 @@
         self.copy_to, self.distances, self.steps = copy_to, distances, steps
         self.whole = lambda: copy(slots, slots, peer)
 
-    def start(self, first=0, last=None):
+    def start(self):
         if self.steps is None:
             for d in self.distances:
                 self.copy_to(d).start()
         else:
-            steps = (self.steps if last is None else last) - first
-            loop(steps, lambda k: self.copy_to(self.distances(k + first)).start())
+            loop(self.steps, lambda k: self.copy_to(self.distances(k)).start())
         return self
 
     def arrive(self):
@@ -114,6 +113,8 @@
     wu,
     wd,
     abuf,
+    psend,
+    precv,
     qsend,
     qbuf,
     lined_s,
@@ -219,21 +220,34 @@
     ld_wv.wait()
     proj = dot(scaled, wp[...])
     square = to_lanes(jnp.sum(block * block, axis=1, keepdims=True))
+    key_at, value_at, last_at = heads * rows, (heads + 1) * rows, (heads + 2) * rows
+    for g in range(heads + 2):
+        psend[0, g * rows : (g + 1) * rows, :] = proj[:, g * LANES : (g + 1) * LANES].astype(BF16)
+    psend[0, last_at:, :] = stacked(three(square)).astype(BF16)
+    odd = lax.rem(z, 2)
+    partner = lax.rem(KV + 1 - 2 * odd, KV)
+    spread(
+        lambda peer: psend.at[0], precv.at[0], precv, send_sem.at[0], recv_sem.at[9], "kv", [partner]
+    ).start().arrive()
+    pair = psend[0].astype(F32) + precv[0].astype(F32)
+    square = pair[last_at : last_at + 1] + pair[last_at + 1 : last_at + 2]
+    square = square + pair[last_at + 2 : last_at + 3]
     extra = stacked((square, square, *three(square)))
     at = iota((8, LANES), 0)
+    queries = pair[0:key_at].astype(BF16)
     for j in range(KV):
-        for g in range(heads):
-            qsend[j, g * rows : (g + 1) * rows, :] = proj[:, g * LANES : (g + 1) * LANES].astype(BF16)
-        key_row = proj[j : j + 1, qcols : qcols + LANES]
-        value_row = proj[j : j + 1, qcols + LANES :]
+        qsend[j, 0:key_at, :] = queries
+        key_row = pair[key_at + j : key_at + j + 1]
+        value_row = pair[value_at + j : value_at + j + 1]
         last = jnp.where(at == 0, key_row, jnp.where(at == 1, value_row, extra))
-        qsend[j, heads * rows :, :] = last.astype(BF16)
-    qbuf[z] = qsend[z]
-    q_copies = spread(lambda peer: qsend.at[peer], qbuf.at[z], qbuf, send_sem.at[0], recv_sem.at[1], "kv")
-    far = KV // 2 - 1
-    q_copies.start(far)
+        qsend[j, key_at:, :] = last.astype(BF16)
+    pairs = z // 2
+    qbuf[pairs] = qsend[z]
     pl.semaphore_wait(ring_sem.at[1], 2)
-    q_copies.start(0, far)
+    reach = [lax.rem(KV + (2 * odd - 1) * d, KV) for d in range(KV // 2 - 1, 0, -1)]
+    q_copies = spread(
+        lambda peer: qsend.at[peer], qbuf.at[pairs], qbuf, send_sem.at[0], recv_sem.at[1], "kv", reach
+    ).start()
     ld_keys = load(keys_h, keys, 0)
     ld_values = load(values_h, values, 1)
     ld_lam = load(lam_h, lam, 2)
@@ -244,7 +258,7 @@
     ld_wd = load(wd_h, wd, 7)
     q_copies.arrive()
     q_sum = qbuf[0].astype(F32)
-    for j in range(1, KV):
+    for j in range(1, KV // 2):
         q_sum = q_sum + qbuf[j].astype(F32)
     r_sum = q_sum[heads * rows :]
     inv_lanes = lax.rsqrt((r_sum[2:3] + r_sum[3:4] + r_sum[4:5]) / D + EPS)
@@ -458,8 +472,9 @@
             pltpu.VMEM(up_weight.shape, BF16),
             pltpu.VMEM(down_weight.shape, BF16),
             pltpu.VMEM((TP, rows, LANES), BF16),
+            *[pltpu.VMEM((1, rows * (qcols // LANES + 2) + 8, LANES), BF16)] * 2,
             pltpu.VMEM((KV, rows * qcols // LANES + 8, LANES), BF16),
-            pltpu.VMEM((KV, rows * qcols // LANES + 8, LANES), BF16),
+            pltpu.VMEM((KV // 2, rows * qcols // LANES + 8, LANES), BF16),
             pltpu.VMEM((lines, LANES), F32),
             pltpu.VMEM((4, lines // 4 + 8, LANES), BF16),
             pltpu.VMEM((KV, lines // 4 + 8, LANES), BF16),
@@ -474,7 +489,7 @@
             pltpu.SemaphoreType.REGULAR((2,)),
             dma((8,)),
             dma((2,)),
-            dma((9,)),
+            dma((10,)),
         ],
         compiler_params=pltpu.CompilerParams(
             collective_id=0, has_side_effects=True, vmem_limit_bytes=64 * 1000 * 1000

time: 78.5 us -> 77.3 us (0.985)
  Pallas kernels: 77.1 us -> 75.8 us
    pallas_call x1, Pallas kernels: 77.1 us -> 75.8 us  [body(): pl.pallas_call(functools.partial(kernel, KV, TP), out_shape=jax.ShapeDtyp...]
where the time goes in v9:
time: 77.3 us; the launch traced here: 77.1 us
  Pallas kernels  75.8 us (98%)
  local copies, waits for them, and re-layouts  1.28 us (2%)
    pallas_call x1, Pallas kernels, body(): pl.pallas_call(functools.partial(kernel, KV, TP), out_shape=jax.ShapeDtyp...  75.8 us

profile of v9, /device:TPU:33, one launch (start us, length us, event | category | flops | bytes accessed | tf_op | source)
XLA Modules:
  0.0 77.1 jit_solution(16748472197881853463)
XLA Ops:
  0.0 75.8 %layer.1 = bf16[16,32]{1,0:T(8,128)(2,1)} custom-call(bf16[16,32]{1,0:T(8,128)(2,1)} %res_h.1, bf16[16,1024,128]{2,1,0:T(8,128)(2,1)} %bitcast.6, bf16[16,1024,128]{2,1,0:T(8,128)(2,1)} %bitcast.7, bf16[2,128]{1,0:T(2,128)(2,1)} %bitcast.8, bf16[256,256]{1,0:T(8,128)(2,1)} %wq_h.1, bf16[256,128]{1,0:T(8,128)(2,1)} %wk_h.1, bf16[256,128]{1,0:T(8,128)(2,1)} %wv_h.1, ...), custom_call_target="tpu_custom_call" | custom-call | tf_op jit(solution)/shard_map/layer/pallas_call | solution.py:457
  75.8 1.3 %copy.15 = bf16[16,32]{1,0:T(8,128)(2,1)} copy(bf16[16,32]{1,0:T(8,128)(2,1)} %layer.1) | data formatting | bytes 2048
